TPU v7x, 128 devices: a whole 4x4x4 slice. The times are simulated.
128 devices in a mesh: sp: 32 (over z, y, core), tp: 4 (over x).
Axes of the slice: x: 4, y: 4, z: 4, core: 2. Of those that a mesh axis runs over, the one named last changes fastest.
Arguments:
- queries_nope: bfloat16 [12288, 8, 128], P('sp', 'tp'), may hold values from -9 to 9
- queries_rope: bfloat16 [12288, 8, 64], P('sp', 'tp'), may hold values from -6 to 6
- latent: bfloat16 [12288, 512], P('sp'), may hold values from -8 to 8, as said below
- rope_key: bfloat16 [12288, 64], P('sp'), may hold values from -6 to 6
- latent_gain: float32 [512], replicated, may hold values from 0.1 to 1.9
- key_up: bfloat16 [512, 1024], P(None, 'tp'), may hold values from -0.25 to 0.25
- value_up: bfloat16 [512, 1024], P(None, 'tp'), may hold values from -0.25 to 0.25
- out_proj: bfloat16 [1024, 2048], P('tp'), may hold values from -0.75 to 0.75
- stream: bfloat16 [12288, 2048], P(('sp', 'tp')), may hold values from -6 to 6
- mix_gain: float32 [2048], replicated, may hold values from 0.1 to 1.9
- w_gate: bfloat16 [2048, 3072], P('sp', 'tp'), may hold values from -0.125 to 0.125
- w_up: bfloat16 [2048, 3072], P('sp', 'tp'), may hold values from -0.125 to 0.125
- w_down: bfloat16 [3072, 2048], P('tp', 'sp'), may hold values from -0.4375 to 0.4375
- mlp_gain: float32 [2048], replicated, may hold values from 0.1 to 1.9
Outputs:
- result: bfloat16 [12288, 2048], P(('sp', 'tp'))
Inputs may be any that keep to these rules, and one draw needn't show every extreme that they name: latent rows carry a mean vector that changes from one eighth of the sequence to the next.
All inputs are finite; a program needn't handle non-finite values.
Results may differ from a plain program's by a relative error of at most 0.017.
Values may be sent and summed in bfloat16 or wider, within the bound.
A program may use at most 192 MiB of HBM per device.

v0:
```python
import jax
import jax.numpy as jnp
from jax import lax
from jax.sharding import PartitionSpec as P

theta_base = 10000.0
residual_weight = 8.0**0.25
norm_floor = 1.0
big_negative = -1e30


def rows_first(arrays, axis, dims):
    turned = [jnp.moveaxis(a, dim, 0) for a, dim in zip(arrays, dims)]
    both = jnp.concatenate([t.reshape(len(t), -1) for t in turned], axis=1)
    filled, at, gathered = (lax.all_gather(both, axis, axis=0, tiled=True), 0, [])
    for t, dim in zip(turned, dims):
        share = filled[:, at : at + t[0].size].reshape(-1, *t.shape[1:])
        gathered.append(jnp.moveaxis(share, 0, dim))
        at += t[0].size
    return tuple(gathered)


def sent_together(arrays, axis, dim, along):
    both = jnp.concatenate(arrays, axis=along)
    filled, at, gathered = (lax.all_gather(both, axis, axis=dim, tiled=True), 0, [])
    for a in arrays:
        gathered.append(lax.slice_in_dim(filled, at, at + a.shape[along], axis=along))
        at += a.shape[along]
    return tuple(gathered)


def in_order(pieces, dim):
    dims = list(pieces.shape[1:])
    dims[dim] *= pieces.shape[0]
    return jnp.moveaxis(pieces, 0, dim).reshape(dims)


def copy_for_each(x, axis):
    copies = jnp.broadcast_to(x, (lax.axis_size(axis), *x.shape))
    return lax.all_to_all(copies, axis, split_axis=0, concat_axis=0, tiled=True)


def collect(x, axis, dim):
    return in_order(copy_for_each(x, axis), dim)


def cut_along(x, dim, devices):
    before, after = (x.shape[:dim], x.shape[dim + 1 :])
    return jnp.moveaxis(x.reshape(*before, devices, -1, *after), dim, 0)


def sent_and_summed(x, axis, dim):
    devices = lax.axis_size(axis)
    pieces = lax.all_to_all(cut_along(x, dim, devices), axis, 0, 0, tiled=True)
    return jnp.sum(pieces.astype(jnp.float32), axis=0)


def rotate(vector, first_row):
    half = vector.shape[-1] // 2
    rates = theta_base ** (-2.0 * jnp.arange(half, dtype=jnp.float32) / vector.shape[-1])
    places = (first_row + jnp.arange(vector.shape[0], dtype=jnp.int32)).astype(jnp.float32)
    angle = places[:, None] * rates[None, :]
    angle = angle.reshape((vector.shape[0],) + (1,) * (vector.ndim - 2) + (half,))
    cosine = jnp.cos(angle)
    sine = jnp.sin(angle)
    left = vector[..., :half]
    right = vector[..., half:]
    return jnp.concatenate([left * cosine - right * sine, left * sine + right * cosine], axis=-1)


def latent_norm(latent, latent_gain):
    wide = latent.astype(jnp.float32)
    factor = lax.rsqrt(jnp.mean(wide * wide, axis=-1, keepdims=True) + norm_floor)
    return (wide * factor * latent_gain).astype(jnp.bfloat16)


def layer_norm(values, gain):
    centre = jnp.mean(values, axis=-1, keepdims=True)
    centred = values - centre
    spread = jnp.mean(centred * centred, axis=-1, keepdims=True)
    return centred * lax.rsqrt(spread + norm_floor) * gain


def per_device(
    queries_nope,
    queries_rope,
    latent,
    rope_key,
    latent_gain,
    key_up,
    value_up,
    out_proj,
    stream,
    mix_gain,
    w_gate,
    w_up,
    w_down,
    mlp_gain,
):
    row_count, head_count, head_dim = queries_nope.shape
    rope_dim = queries_rope.shape[2]
    first_row = lax.axis_index("sp") * row_count
    query_turned = rotate(queries_rope.astype(jnp.float32), first_row).astype(jnp.bfloat16)
    key_turned = rotate(rope_key.astype(jnp.float32), first_row).astype(jnp.bfloat16)
    normed = latent_norm(latent, latent_gain)
    gate_full, up_full, down_full = rows_first((w_gate, w_up, w_down), "sp", (0, 0, 1))
    scale = (head_dim + rope_dim) ** (-0.5)
    query_places = first_row + jnp.arange(row_count, dtype=jnp.int32)
    last_place = first_row + row_count - 1

    def add_piece(carry, piece):
        top, denominators, weighted = carry
        latent_piece, rotary_piece = piece
        count = latent_piece.shape[0]
        keys = jnp.dot(latent_piece, key_up, preferred_element_type=jnp.float32).astype(
            jnp.bfloat16
        )
        keys = keys.reshape(count, head_count, head_dim)
        values_here = jnp.dot(latent_piece, value_up, preferred_element_type=jnp.float32).astype(
            jnp.bfloat16
        )
        values_here = values_here.reshape(count, head_count, head_dim)
        score = jnp.einsum("thd,shd->hts", queries_nope, keys, preferred_element_type=jnp.float32)
        score = score + jnp.einsum(
            "thr,sr->hts", query_turned, rotary_piece, preferred_element_type=jnp.float32
        )
        score = score * scale
        allowed = jnp.arange(count, dtype=jnp.int32)[None, :] <= query_places[:, None]
        score = jnp.where(allowed[None], score, big_negative)
        new_top = jnp.maximum(top, jnp.max(score, axis=2))
        powers = jnp.exp(score - new_top[:, :, None]) * allowed[None]
        shrink = jnp.exp(top - new_top)
        denominators = jnp.sum(powers, axis=2)
        weighted = weighted * shrink.T[:, :, None] + jnp.einsum(
            "hts,shd->thd",
            powers.astype(jnp.bfloat16),
            values_here,
            preferred_element_type=jnp.float32,
        )
        return (new_top, denominators, weighted)

    start_state = (
        jnp.full((head_count, row_count), big_negative, jnp.float32),
        jnp.zeros((head_count, row_count), jnp.float32),
        jnp.zeros((row_count, head_count, head_dim), jnp.float32),
    )
    piece = sent_together((normed, key_turned), "sp", 0, 1)
    top, denominators, weighted = lax.cond(
        jnp.int32(0) <= last_place,
        lambda state: add_piece(state, piece),
        lambda state: state,
        start_state,
    )
    attended = (
        (weighted / denominators.T[:, :, None])
        .astype(jnp.bfloat16)
        .reshape(row_count, head_count * head_dim)
    )
    row_heads = lax.all_to_all(attended, "tp", split_axis=0, concat_axis=1, tiled=True)
    whole_proj = collect(out_proj, "tp", 0)
    projected = jnp.dot(row_heads, whole_proj, preferred_element_type=jnp.float32)
    mixed = layer_norm(residual_weight * stream.astype(jnp.float32) + projected, mix_gain).astype(
        jnp.bfloat16
    )
    expand_piece = collect(mixed, "tp", 0)
    gate_sum = jnp.dot(expand_piece, gate_full, preferred_element_type=jnp.float32)
    up_sum = jnp.dot(expand_piece, up_full, preferred_element_type=jnp.float32)
    hidden = (jax.nn.silu(gate_sum) * up_sum).astype(jnp.bfloat16)
    lowered = sent_and_summed(
        jnp.dot(hidden, down_full, preferred_element_type=jnp.float32).astype(jnp.bfloat16), "tp", 0
    )
    return layer_norm(residual_weight * mixed.astype(jnp.float32) + 0.5 * lowered, mlp_gain).astype(
        jnp.bfloat16
    )


def solution(mesh):
    return jax.shard_map(
        per_device,
        mesh=mesh,
        in_specs=(
            P("sp", "tp", None),
            P("sp", "tp", None),
            P("sp", None),
            P("sp", None),
            P(),
            P(None, "tp"),
            P(None, "tp"),
            P("tp", None),
            P(("sp", "tp"), None),
            P(),
            P("sp", "tp"),
            P("sp", "tp"),
            P("tp", "sp"),
            P(),
        ),
        out_specs=P(("sp", "tp"), None),
        check_vma=False,
    )
```

profile of v0, /device:TPU:1, one launch (start us, length us, event | category | flops | bytes accessed | tf_op | source)
XLA Modules:
  0.0 285.3 jit_solution(10291751119979963595)
XLA Ops:
  6.5 0.0 copy-start.2
  6.5 0.0 all-gather.3.cloned.1.call-start
  6.6 0.8 convert_element_type.70
  7.4 0.0 copy-start.4
  7.4 1.2 copy.20
  8.7 0.1 fusion.42
  8.8 0.8 fusion.44
  9.6 0.3 multiply_cosine_fusion
  9.9 0.9 pad_maximum_fusion
  10.8 0.0 all-gather.3.cloned.1.call-update
  10.8 0.0 all-gather.5.cloned.1.call-start
  10.8 1.7 pad_maximum_fusion.1
  12.6 0.0 all-gather.5.cloned.1.call-update
  12.6 3.8 %broadcast_in_dim.34 = bf16[4,256,2048]{2,1,0:T(8,128)(2,1)} broadcast(bf16[256,2048]{1,0:T(8,128)(2,1)} %param.23), dimensions={1,2} | broadcast | bytes 5242880 | tf_op jit(solution)/shard_map/broadcast_in_dim | solution.py:39
  16.4 4.8 %all-to-all-start.1 = ((bf16[4,256,2048]{2,1,0:T(8,128)(2,1)}), bf16[4,256,2048]{2,1,0:T(8,128)(2,1)}, u32[]{:S(2)}, u32[]{:S(2)}) async-start(bf16[4,256,2048]{2,1,0:T(8,128)(2,1)} %broadcast_in_dim.34), calls=%async_computation.1 | async-start | bytes 8388608 | tf_op jit(solution)/shard_map/all_to_all | solution.py:40
  21.2 0.0 copy-done.2
  21.3 66.7 %all-gather.3.cloned.1.call-done = bf16[12288,576]{0,1:T(8,128)(2,1)} async-done(((bf16[384,576]{0,1:T(8,128)(2,1)}), bf16[12288,576]{0,1:T(8,128)(2,1)}) %all-gather.3.cloned.1.call-update) | async-done | bytes 14155792 | tf_op jit(solution)/shard_map/all_gather | solution.py:25
  88.0 0.0 copy-done.4
  88.0 117.5 %conditional.1 = (f32[2,384]{1,0:T(2,128)S(1)}, f32[384,2,128]{0,2,1:T(8,128)S(1)}) conditional(s32[]{:T(128)} %convert_element_type.67, () %tuple.13, (s32[]{:T(128)}, s32[384]{0:T(512)S(1)}, bf16[12288,576]{0,1:T(8,128)(2,1)}, bf16[512,256]{1,0:T(8,128)(2,1)S(1)}, bf16[384,2,128]{2,1,0:T(2,128)(2,1)}, /*index=5*/bf16[384,2,64]{0,2,1:T(8,128)(2,1)S(1)}, ...), branch_computations={%region_1.0_spmd, %region_2.5_spmd} | conditional | flops 12592448512 | bytes 308736576 | solution.py:148
  88.0 15.9 %fusion.10 = f32[12288,384,2]{1,0,2:T(8,128)} fusion(bf16[384,2,64]{0,2,1:T(8,128)(2,1)S(1)} %get-tuple-element.29, bf16[12288,576]{0,1:T(8,128)(2,1)} %get-tuple-element.26), kind=kOutput, calls=%fused_computation.14 | convolution fusion | flops 1207959552 | bytes 39419904 | tf_op jit(solution)/shard_map/cond/branch_1_fun/thr,sr->hts/dot_general | solution.py:124
  103.9 10.8 %convolution_convert_fusion.1 = bf16[12288,256]{0,1:T(8,128)(2,1)} fusion(bf16[512,256]{1,0:T(8,128)(2,1)S(1)} %get-tuple-element.38, bf16[12288,576]{0,1:T(8,128)(2,1)} %get-tuple-element.26), kind=kOutput, calls=%fused_computation.11 | convolution fusion | flops 3224371200 | bytes 19136512 | tf_op jit(solution)/shard_map/cond/branch_1_fun/dot_general | solution.py:115
  114.7 7.8 %fusion.19 = (f32[384,12288]{0,1:T(8,128)}, pred[384,12288]{0,1:T(8,128)(4,1)S(1)}) fusion(s32[384]{0:T(512)S(1)} %broadcast_add_fusion), kind=kLoop, calls=%fused_computation.19 | loop fusion | flops 9437184 | bytes 23594496 | tf_op jit(solution)/shard_map/cond/branch_1_fun/convert_element_type | solution.py:131
  122.5 0.0 copy-done
  122.5 31.9 %fusion.49 = (f32[2,384]{1,0:T(2,128)S(1)}, f32[2,384,12288]{1,2,0:T(8,128)}) fusion(f32[12288,384,2]{1,0,2:T(8,128)} %fusion.10, bf16[12288,2,128]{0,2,1:T(8,128)(2,1)} %bitcast.41, bf16[384,2,128]{2,1,0:T(2,128)(2,1)S(1)} %copy-done, pred[384,12288]{0,1:T(8,128)(4,1)S(1)} %get-tuple-element.51), kind=kOutput, calls=%fused_computation.70 | convolution fusion | flops 2453667072 | bytes 86707200 | tf_op jit(solution)/shard_map/cond/branch_1_fun/thd,shd->hts/dot_general | solution.py:123
  154.3 10.7 %convolution_convert_fusion = bf16[12288,256]{0,1:T(8,128)(2,1)} fusion(bf16[512,256]{1,0:T(8,128)(2,1)} %get-tuple-element.40, bf16[12288,576]{0,1:T(8,128)(2,1)} %get-tuple-element.26), kind=kOutput, calls=%fused_computation.10 | convolution fusion | flops 3224371200 | bytes 19136512 | tf_op jit(solution)/shard_map/cond/branch_1_fun/dot_general | solution.py:119
  165.1 21.6 %fusion.16 = f32[384,2,128]{0,2,1:T(8,128)S(1)} fusion(bf16[12288,2,128]{0,2,1:T(8,128)(2,1)} %bitcast.40, f32[2,384,12288]{1,2,0:T(8,128)} %get-tuple-element.53, f32[384,12288]{0,1:T(8,128)} %get-tuple-element.50, f32[2,384]{1,0:T(2,128)S(1)} %get-tuple-element.49, f32[384,2]{0,1:T(2,128)S(1)} %get-tuple-element.48), kind=kOutput, calls=%fused_computation.18 | convolution fusion | flops 2444328960 | bytes 63313920 | tf_op jit(solution)/shard_map/cond/branch_1_fun/hts,shd->thd/dot_general | solution.py:134
  186.7 18.7 %fusion.3 = f32[2,384]{1,0:T(2,128)S(1)} fusion(f32[2,384,12288]{1,2,0:T(8,128)} %get-tuple-element.53, f32[384,12288]{0,1:T(8,128)} %get-tuple-element.50, f32[2,384]{1,0:T(2,128)S(1)} %get-tuple-element.49), kind=kLoop, calls=%fused_computation.5 | loop fusion | flops 28310784 | bytes 56629248 | tf_op jit(solution)/shard_map/cond/branch_1_fun/reduce_sum | solution.py:133
  205.5 0.0 copy-start.1
  205.5 0.2 copy.22
  205.7 0.1 all_to_all.21
  205.8 0.0 all-to-all-done.1
  205.8 9.1 %all_to_all.31 = bf16[4,96,256]{2,1,0:T(8,128)(2,1)S(1)} all-to-all(bf16[4,96,256]{2,1,0:T(8,128)(2,1)S(1)} %all_to_all.21), channel_id=1, replica_groups=mesh['sp'=32,'tp'=4] {'tp'}, dimensions={0} | all-to-all | bytes 393216 | tf_op jit(solution)/shard_map/all_to_all | solution.py:159
  214.9 3.2 %fusion.50 = (f32[96]{0:T(128)S(1)}, f32[96,2048]{1,0:T(8,128)S(1)}) fusion(bf16[4,256,2048]{2,1,0:T(8,128)(2,1)} %all-to-all-done.1, bf16[4,96,256]{2,1,0:T(8,128)(2,1)S(1)} %all_to_all.31, bf16[96,2048]{1,0:T(8,128)(2,1)} %param.24), kind=kOutput, calls=%fused_computation.71 | convolution fusion | flops 403439520 | bytes 5570944 | tf_op jit(solution)/shard_map/dot_general | solution.py:161
  218.1 0.2 multiply_reduce_fusion.1
  218.4 0.0 copy-done.1
  218.4 0.2 multiply_convert_fusion.1
  218.6 1.3 broadcast_in_dim.35
  219.9 3.6 %all-to-all-start.2 = ((bf16[4,96,2048]{2,1,0:T(8,128)(2,1)}), bf16[4,96,2048]{2,1,0:T(8,128)(2,1)S(1)}, u32[]{:S(2)}, u32[]{:S(2)}) async-start(bf16[4,96,2048]{2,1,0:T(8,128)(2,1)} %broadcast_in_dim.35), calls=%async_computation.2 | async-start | bytes 3145728 | tf_op jit(solution)/shard_map/all_to_all | solution.py:40
  223.5 0.0 all-gather.5.cloned.1.call-done
  223.5 19.2 %all-to-all-done.2 = bf16[4,96,2048]{2,1,0:T(8,128)(2,1)S(1)} async-done(((bf16[4,96,2048]{2,1,0:T(8,128)(2,1)}), bf16[4,96,2048]{2,1,0:T(8,128)(2,1)S(1)}, u32[]{:S(2)}, u32[]{:S(2)}) %all-to-all-start.2) | async-done | bytes 1572896 | tf_op jit(solution)/shard_map/all_to_all | solution.py:40
  242.7 4.3 %fusion.25 = f32[384,768]{1,0:T(8,128)} fusion(bf16[384,2048]{1,0:T(8,128)(2,1)S(1)} %bitcast.42, bf16[2048,2304]{1,0:T(8,128)(2,1)} %all-gather.5.cloned.1.call-done), kind=kOutput, calls=%fused_computation.28 | convolution fusion | flops 1207959552 | bytes 5898240 | tf_op jit(solution)/shard_map/dot_general | solution.py:166
  247.0 7.4 %fusion.27 = bf16[384,2048]{1,0:T(8,128)(2,1)} fusion(bf16[2048,2304]{1,0:T(8,128)(2,1)} %all-gather.5.cloned.1.call-done, bf16[384,2048]{1,0:T(8,128)(2,1)S(1)} %bitcast.43, f32[384,768]{1,0:T(8,128)} %fusion.25), kind=kOutput, calls=%fused_computation.31 | convolution fusion | flops 2418475008 | bytes 10616832 | tf_op jit(solution)/shard_map/dot_general | solution.py:170
  254.4 21.9 %all_to_all.32 = bf16[4,96,2048]{2,1,0:T(8,128)(2,1)S(1)} all-to-all(bf16[4,96,2048]{2,1,0:T(8,128)(2,1)} %bitcast.44), channel_id=1, replica_groups=mesh['sp'=32,'tp'=4] {'tp'}, dimensions={0} | all-to-all | bytes 3145728 | tf_op jit(solution)/shard_map/all_to_all | solution.py:54
  276.3 0.3 convert_reduce_fusion
  276.5 0.3 fusion.47
  276.9 0.4 multiply_reduce_fusion
  277.3 0.0 copy-done.3
  277.3 1.2 multiply_convert_fusion
  (16 shorter events, 0.2 us)
Async XLA Ops:
  6.5 14.7 %copy-start.2 = (bf16[384,2,64]{0,2,1:T(8,128)(2,1)S(1)}, bf16[384,2,64]{0,2,1:T(8,128)(2,1)}, u32[]{:S(2)}) copy-start(bf16[384,2,64]{0,2,1:T(8,128)(2,1)} %param.17) | copy-start | bytes 294916
  6.5 81.4 %all-gather.3.cloned.1.call-start = ((), (), s32[]{:S(2)}) async-start(), calls=%async_computation.4 | async-start | bytes 14598144 | tf_op jit(solution)/shard_map/all_gather | solution.py:25
  7.4 80.6 %copy-start.4 = (bf16[512,256]{1,0:T(8,128)(2,1)S(1)}, bf16[512,256]{1,0:T(8,128)(2,1)}, u32[]{:S(2)}) copy-start(bf16[512,256]{1,0:T(8,128)(2,1)} %param.21) | copy-start | bytes 786436
  10.8 212.7 %all-gather.5.cloned.1.call-start = ((), (), s32[]{:S(2)}) async-start(), calls=%async_computation.5 | async-start | bytes 9732096 | tf_op jit(solution)/shard_map/all_gather | solution.py:15
  16.4 189.5 %all-to-all-start.1 = ((bf16[4,256,2048]{2,1,0:T(8,128)(2,1)}), bf16[4,256,2048]{2,1,0:T(8,128)(2,1)}, u32[]{:S(2)}, u32[]{:S(2)}) async-start(bf16[4,256,2048]{2,1,0:T(8,128)(2,1)} %broadcast_in_dim.34), calls=%async_computation.1 | async-start | bytes 8388608 | tf_op jit(solution)/shard_map/all_to_all | solution.py:40
  114.7 7.8 %copy-start = (bf16[384,2,128]{2,1,0:T(2,128)(2,1)S(1)}, bf16[384,2,128]{2,1,0:T(2,128)(2,1)}, u32[]{:S(2)}) copy-start(bf16[384,2,128]{2,1,0:T(2,128)(2,1)} %get-tuple-element.45) | copy-start | bytes 589828 | tf_op jit(solution)/shard_map/cond
  205.5 12.9 %copy-start.1 = (f32[2048]{0:T(1024)S(1)}, f32[2048]{0:T(1024)}, u32[]{:S(2)}) copy-start(f32[2048]{0:T(1024)} %param.25) | copy-start | bytes 24580
  219.9 22.7 %all-to-all-start.2 = ((bf16[4,96,2048]{2,1,0:T(8,128)(2,1)}), bf16[4,96,2048]{2,1,0:T(8,128)(2,1)S(1)}, u32[]{:S(2)}, u32[]{:S(2)}) async-start(bf16[4,96,2048]{2,1,0:T(8,128)(2,1)} %broadcast_in_dim.35), calls=%async_computation.2 | async-start | bytes 3145728 | tf_op jit(solution)/shard_map/all_to_all | solution.py:40
  247.0 30.3 %copy-start.3 = (f32[2048]{0:T(1024)S(1)}, f32[2048]{0:T(1024)}, u32[]{:S(2)}) copy-start(f32[2048]{0:T(1024)} %param.29) | copy-start | bytes 24580
Sparse Core Ops, SparseCore 0:
  10.9 77.0 all-gather.2
  90.2 55.1 all-gather.4
where the time goes:
time: 288 us; the launch traced here: 285 us
  matrix products  106 us (37%)
  waiting for transfers between devices  85.9 us (30%)
  other arithmetic  33.9 us (12%)
  blocking collectives  31 us (11%)
  between operations  13.6 us (5%)
  starting transfers between devices  8.44 us (3%)
  local copies, waits for them, and re-layouts  6.68 us (2%)
    all_gather x1, waiting for transfers between devices, sent_together(): lax.all_gather(both, axis, axis=dim, tiled=True)  66.7 us
    dot_general x1, matrix products, add_piece(): jnp.einsum('thd,shd->hts', queries_nope, keys, preferred_element_type=jnp...  31.9 us
    all_to_all x1, blocking collectives, sent_and_summed(): pieces = lax.all_to_all(cut_along(x, dim, devices), axis, 0, 0, tiled=True)  21.9 us
    dot_general x1, matrix products, add_piece(): jnp.einsum('hts,shd->thd', powers.astype(jnp.bfloat16), values_here, pref...  21.6 us
    all_to_all x2, waiting for transfers between devices, copy_for_each(): return lax.all_to_all(copies, axis, split_axis=0, concat_axis=0, tiled=True)  19.2 us
    reduce_sum x1, other arithmetic, add_piece(): denominators = jnp.sum(powers, axis=2)  18.7 us
    dot_general x1, matrix products, add_piece(): jnp.einsum('thr,sr->hts', query_turned, rotary_piece, preferred_element_t...  15.9 us
    dot_general x1, matrix products, add_piece(): jnp.dot(latent_piece, key_up, preferred_element_type=jnp.float32)  10.8 us
  transfers between devices with their start and end apart: 4, of which 2 were waited for; matrix products, arithmetic and copies ran while one was open for 45% of the time, Pallas kernels for 0%

commit v1 on v0

v1 whole, which is shorter than its diff:
```python
import functools
import math

import jax
import jax.numpy as jnp
from jax import lax
from jax.experimental import pallas as pl
from jax.experimental.pallas import tpu as pltpu
from jax.sharding import PartitionSpec as P

theta_base = 10000.0
residual_weight = 8.0**0.25
norm_floor = 1.0
big_negative = -1e30
F32 = jnp.float32
BF16 = jnp.bfloat16


def rows_first(arrays, axis, dims):
    turned = [jnp.moveaxis(a, dim, 0) for a, dim in zip(arrays, dims)]
    both = jnp.concatenate([t.reshape(len(t), -1) for t in turned], axis=1)
    filled, at, gathered = (lax.all_gather(both, axis, axis=0, tiled=True), 0, [])
    for t, dim in zip(turned, dims):
        share = filled[:, at : at + t[0].size].reshape(-1, *t.shape[1:])
        gathered.append(jnp.moveaxis(share, 0, dim))
        at += t[0].size
    return tuple(gathered)


def in_order(pieces, dim):
    dims = list(pieces.shape[1:])
    dims[dim] *= pieces.shape[0]
    return jnp.moveaxis(pieces, 0, dim).reshape(dims)


def copy_for_each(x, axis):
    copies = jnp.broadcast_to(x, (lax.axis_size(axis), *x.shape))
    return lax.all_to_all(copies, axis, split_axis=0, concat_axis=0, tiled=True)


def collect(x, axis, dim):
    return in_order(copy_for_each(x, axis), dim)


def cut_along(x, dim, devices):
    before, after = (x.shape[:dim], x.shape[dim + 1 :])
    return jnp.moveaxis(x.reshape(*before, devices, -1, *after), dim, 0)


def sent_and_summed(x, axis, dim):
    devices = lax.axis_size(axis)
    pieces = lax.all_to_all(cut_along(x, dim, devices), axis, 0, 0, tiled=True)
    return jnp.sum(pieces.astype(jnp.float32), axis=0)


def rotate(vector, first_row):
    half = vector.shape[-1] // 2
    rates = theta_base ** (-2.0 * jnp.arange(half, dtype=jnp.float32) / vector.shape[-1])
    places = (first_row + jnp.arange(vector.shape[0], dtype=jnp.int32)).astype(jnp.float32)
    angle = places[:, None] * rates[None, :]
    angle = angle.reshape((vector.shape[0],) + (1,) * (vector.ndim - 2) + (half,))
    cosine = jnp.cos(angle)
    sine = jnp.sin(angle)
    left = vector[..., :half]
    right = vector[..., half:]
    return jnp.concatenate([left * cosine - right * sine, left * sine + right * cosine], axis=-1)


def latent_norm(latent, latent_gain):
    wide = latent.astype(jnp.float32)
    factor = lax.rsqrt(jnp.mean(wide * wide, axis=-1, keepdims=True) + norm_floor)
    return (wide * factor * latent_gain).astype(jnp.bfloat16)


def layer_norm(values, gain):
    centre = jnp.mean(values, axis=-1, keepdims=True)
    centred = values - centre
    spread = jnp.mean(centred * centred, axis=-1, keepdims=True)
    return centred * lax.rsqrt(spread + norm_floor) * gain


def attend_chunk(kv, q_ref, m_ref, l_ref, acc_ref, rows, const, diag):
    half = rows // 2
    blocks = rows // 128
    r = kv[4 * rows : 4 * rows + half, :]
    for h in range(2):
        top = jnp.concatenate([kv[h * rows : h * rows + half, :], r], axis=1)
        low = jnp.concatenate([kv[h * rows + half : (h + 1) * rows, :], r], axis=1)
        s = jnp.concatenate(
            [
                jnp.dot(top, q_ref[2 * h], preferred_element_type=F32),
                jnp.dot(low, q_ref[2 * h + 1], preferred_element_type=F32),
            ],
            axis=0,
        )
        s = s * const
        if diag:
            key = lax.broadcasted_iota(jnp.int32, s.shape, 0)
            query = lax.broadcasted_iota(jnp.int32, s.shape, 1)
            s = jnp.where(key <= query, s, big_negative)
        m_old = m_ref[h]
        m_new = jnp.maximum(m_old, jnp.max(s, axis=0, keepdims=True))
        p = jnp.exp2(s - m_new)
        alpha = jnp.exp2(m_old - m_new)
        l_ref[h] = l_ref[h] * alpha + jnp.sum(p, axis=0, keepdims=True)
        m_ref[h] = m_new
        at = 2 * rows + h * rows
        vt = jnp.concatenate([kv[at + 128 * i : at + 128 * (i + 1), :] for i in range(blocks)], axis=1)
        acc_ref[h] = acc_ref[h] * alpha + jnp.dot(vt, p.astype(BF16), preferred_element_type=F32)


def attention_kernel(rows, const, kv_ref, q_ref, out_ref, m_ref, l_ref, acc_ref):
    me = lax.axis_index("sp")
    m_ref[...] = jnp.full_like(m_ref, big_negative)
    l_ref[...] = jnp.zeros_like(l_ref)
    acc_ref[...] = jnp.zeros_like(acc_ref)
    attend_chunk(kv_ref.at[me], q_ref, m_ref, l_ref, acc_ref, rows, const, True)

    def step(j, _):
        attend_chunk(kv_ref.at[j], q_ref, m_ref, l_ref, acc_ref, rows, const, False)
        return _

    lax.fori_loop(0, me, step, 0)
    for h in range(2):
        out_ref[:, 128 * h : 128 * (h + 1)] = (acc_ref[h] / l_ref[h]).T.astype(BF16)


def per_device(
    queries_nope,
    queries_rope,
    latent,
    rope_key,
    latent_gain,
    key_up,
    value_up,
    out_proj,
    stream,
    mix_gain,
    w_gate,
    w_up,
    w_down,
    mlp_gain,
):
    rows, heads, head_dim = queries_nope.shape
    rope_dim = queries_rope.shape[2]
    first_row = lax.axis_index("sp") * rows
    query_turned = rotate(queries_rope.astype(F32), first_row).astype(BF16)
    key_turned = rotate(rope_key.astype(F32), first_row).astype(BF16)
    normed = latent_norm(latent, latent_gain)
    keys = jnp.dot(normed, key_up, preferred_element_type=F32).astype(BF16)
    values_t = lax.dot_general(
        value_up, normed, (((0,), (1,)), ((), ())), preferred_element_type=F32
    ).astype(BF16)
    half = rows // 2
    slab = jnp.concatenate(
        [keys[:, :128], keys[:, 128:]]
        + [values_t[128 * h : 128 * (h + 1), 128 * i : 128 * (i + 1)] for h in range(2) for i in range(rows // 128)]
        + [jnp.concatenate([key_turned[:half], key_turned[half:]], axis=1)],
        axis=0,
    )
    pieces = lax.all_gather(slab, "sp", axis=0, tiled=False)
    gate_full, up_full, down_full = rows_first((w_gate, w_up, w_down), "sp", (0, 0, 1))
    qn = jnp.transpose(queries_nope, (1, 2, 0))
    qr = jnp.transpose(query_turned, (1, 2, 0))
    zero = jnp.zeros_like(qr)
    q_all = jnp.stack(
        [jnp.concatenate([qn, qr, zero], axis=1), jnp.concatenate([qn, zero, qr], axis=1)], axis=1
    ).reshape(2 * heads, 2 * head_dim, rows)
    const = (head_dim + rope_dim) ** (-0.5) * math.log2(math.e)
    attended = pl.pallas_call(
        functools.partial(attention_kernel, rows, const),
        out_shape=jax.ShapeDtypeStruct((rows, heads * head_dim), BF16),
        in_specs=[pl.BlockSpec(memory_space=pltpu.VMEM)] * 2,
        out_specs=pl.BlockSpec(memory_space=pltpu.VMEM),
        scratch_shapes=[
            pltpu.VMEM((2, 1, rows), F32),
            pltpu.VMEM((2, 1, rows), F32),
            pltpu.VMEM((2, 128, rows), F32),
        ],
        compiler_params=pltpu.CompilerParams(vmem_limit_bytes=48 * 1024 * 1024),
        cost_estimate=pl.CostEstimate(flops=10**10, bytes_accessed=15 * 10**6, transcendentals=10**7),
        name="attend",
    )(pieces, q_all)
    row_heads = lax.all_to_all(attended, "tp", split_axis=0, concat_axis=1, tiled=True)
    whole_proj = collect(out_proj, "tp", 0)
    projected = jnp.dot(row_heads, whole_proj, preferred_element_type=F32)
    mixed = layer_norm(residual_weight * stream.astype(F32) + projected, mix_gain).astype(BF16)
    expand_piece = collect(mixed, "tp", 0)
    gate_sum = jnp.dot(expand_piece, gate_full, preferred_element_type=F32)
    up_sum = jnp.dot(expand_piece, up_full, preferred_element_type=F32)
    hidden = (jax.nn.silu(gate_sum) * up_sum).astype(BF16)
    lowered = sent_and_summed(
        jnp.dot(hidden, down_full, preferred_element_type=F32).astype(BF16), "tp", 0
    )
    return layer_norm(residual_weight * mixed.astype(F32) + 0.5 * lowered, mlp_gain).astype(BF16)


def solution(mesh):
    return jax.shard_map(
        per_device,
        mesh=mesh,
        in_specs=(
            P("sp", "tp", None),
            P("sp", "tp", None),
            P("sp", None),
            P("sp", None),
            P(),
            P(None, "tp"),
            P(None, "tp"),
            P("tp", None),
            P(("sp", "tp"), None),
            P(),
            P("sp", "tp"),
            P("sp", "tp"),
            P("tp", "sp"),
            P(),
        ),
        out_specs=P(("sp", "tp"), None),
        check_vma=False,
    )
```

time: 288 us -> 199 us (0.69)
  the two profiles are of different devices: /device:TPU:1 before, /device:TPU:120 now
where the time goes in v1:
time: 199 us; the launch traced here: 198 us
  waiting for transfers between devices  74.8 us (38%)
  blocking collectives  35.2 us (18%)
  Pallas kernels  34.6 us (17%)
  matrix products  17.9 us (9%)
  between operations  13.8 us (7%)
  starting transfers between devices  8.59 us (4%)
  other arithmetic  7.38 us (4%)
  local copies, waits for them, and re-layouts  5.94 us (3%)
    all_gather x1, waiting for transfers between devices, per_device(): pieces = lax.all_gather(slab, 'sp', axis=0, tiled=False)  53.7 us
    pallas_call x1, Pallas kernels, per_device(): pl.pallas_call(functools.partial(attention_kernel, rows, const), out_shap...  34.6 us
    all_to_all x1, blocking collectives, sent_and_summed(): pieces = lax.all_to_all(cut_along(x, dim, devices), axis, 0, 0, tiled=True)  23.8 us
    all_to_all x2, waiting for transfers between devices, copy_for_each(): return lax.all_to_all(copies, axis, split_axis=0, concat_axis=0, tiled=True)  18.7 us
    all_to_all x1, blocking collectives, per_device(): lax.all_to_all(attended, 'tp', split_axis=0, concat_axis=1, tiled=True)  11.4 us
    all_to_all x2, starting transfers between devices, copy_for_each(): return lax.all_to_all(copies, axis, split_axis=0, concat_axis=0, tiled=True)  8.54 us
    dot_general x1, matrix products, per_device(): jnp.dot(hidden, down_full, preferred_element_type=F32).astype(BF16)  7.41 us
    dot_general x1, matrix products, per_device(): gate_sum = jnp.dot(expand_piece, gate_full, preferred_element_type=F32)  4.31 us
  transfers between devices with their start and end apart: 4, of which 3 were waited for; matrix products, arithmetic and copies ran while one was open for 6% of the time, Pallas kernels for 17%

profile of v1, /device:TPU:120, one launch (start us, length us, event | category | flops | bytes accessed | tf_op | source)
XLA Modules:
  0.0 198.2 jit_solution(2001040852424493183)
XLA Ops:
  6.5 0.0 copy-start
  6.5 0.0 all-gather.6.cloned.1.call-start
  6.6 0.0 copy-start.10
  6.6 1.2 fusion.22
  7.8 0.0 copy-done
  7.8 1.4 fusion.21
  9.2 0.0 copy-start.6
  9.2 0.0 copy-start.7
  9.2 0.0 copy-start.8
  9.2 1.5 convolution_convert_fusion.1
  10.7 0.0 copy-start.1
  10.9 0.3 multiply_cosine_fusion
  11.2 0.1 fusion.30
  11.3 0.1 copy.21
  11.4 0.0 copy-start.2
  11.4 0.8 copy-done.2
  12.2 0.0 all-gather.6.cloned.1.call-update
  12.2 0.0 all-gather.4.cloned.1.call-start
  12.3 0.7 pad_maximum_fusion.1
  13.0 0.0 all-gather.4.cloned.1.call-update
  13.0 2.6 %broadcast_in_dim.7 = bf16[4,256,2048]{2,1,0:T(8,128)(2,1)} broadcast(bf16[256,2048]{1,0:T(8,128)(2,1)S(1)} %copy-done.1), dimensions={1,2} | broadcast | bytes 5242880 | tf_op jit(solution)/shard_map/broadcast_in_dim | solution.py:37
  15.6 5.0 %all-to-all-start.1 = ((bf16[4,256,2048]{2,1,0:T(8,128)(2,1)}), bf16[4,256,2048]{2,1,0:T(8,128)(2,1)}, u32[]{:S(2)}, u32[]{:S(2)}) async-start(bf16[4,256,2048]{2,1,0:T(8,128)(2,1)} %broadcast_in_dim.7), calls=%async_computation.1 | async-start | bytes 8388608 | tf_op jit(solution)/shard_map/all_to_all | solution.py:38
  20.7 0.2 copy.22
  20.9 0.1 broadcast_in_dim.6
  21.0 1.3 maximum_bitcast_fusion
  22.3 1.1 pad_maximum_fusion
  23.5 0.7 copy.24
  24.2 53.7 %all-gather.6.cloned.1.call-done = bf16[55296,128]{1,0:T(8,128)(2,1)} async-done(((bf16[1728,128]{1,0:T(8,128)(2,1)}), bf16[55296,128]{1,0:T(8,128)(2,1)}) %all-gather.6.cloned.1.call-update) | async-done | bytes 14155792 | tf_op jit(solution)/shard_map/all_gather | solution.py:161
  77.8 34.6 %attend.1 = bf16[384,256]{1,0:T(8,128)(2,1)S(1)} custom-call(bf16[32,1728,128]{2,1,0:T(8,128)(2,1)} %bitcast.36, bf16[4,256,384]{2,1,0:T(8,128)(2,1)S(1)} %bitcast.29), custom_call_target="tpu_custom_call" | custom-call | flops 10000000000 | bytes 15000000 | tf_op jit(solution)/shard_map/attend/pallas_call | solution.py:170
  112.4 0.0 all-to-all-done.1
  112.4 11.4 %all_to_all.31 = bf16[4,96,256]{2,1,0:T(8,128)(2,1)S(1)} all-to-all(bf16[4,96,256]{2,1,0:T(8,128)(2,1)S(1)} %bitcast.30), channel_id=1, replica_groups=mesh['sp'=32,'tp'=4] {'tp'}, dimensions={0} | all-to-all | bytes 393216 | tf_op jit(solution)/shard_map/all_to_all | solution.py:184
  123.8 3.3 %fusion.33 = (f32[96]{0:T(128)S(1)}, f32[96,2048]{1,0:T(8,128)S(1)}) fusion(bf16[4,256,2048]{2,1,0:T(8,128)(2,1)} %all-to-all-done.1, bf16[4,96,256]{2,1,0:T(8,128)(2,1)S(1)} %all_to_all.31, bf16[96,2048]{1,0:T(8,128)(2,1)S(1)} %copy-done.3), kind=kOutput, calls=%fused_computation.64 | convolution fusion | flops 403439520 | bytes 5570944 | tf_op jit(solution)/shard_map/dot_general | solution.py:186
  127.2 0.2 multiply_reduce_fusion.1
  127.4 0.0 copy-done.5
  127.4 0.2 multiply_convert_fusion.1
  127.6 1.3 broadcast_in_dim.8
  129.0 3.6 %all-to-all-start.2 = ((bf16[4,96,2048]{2,1,0:T(8,128)(2,1)}), bf16[4,96,2048]{2,1,0:T(8,128)(2,1)S(1)}, u32[]{:S(2)}, u32[]{:S(2)}) async-start(bf16[4,96,2048]{2,1,0:T(8,128)(2,1)} %broadcast_in_dim.8), calls=%async_computation.2 | async-start | bytes 3145728 | tf_op jit(solution)/shard_map/all_to_all | solution.py:38
  132.5 2.4 %all-gather.4.cloned.1.call-done = bf16[2048,2304]{1,0:T(8,128)(2,1)} async-done(((bf16[64,2304]{1,0:T(8,128)(2,1)}), bf16[2048,2304]{1,0:T(8,128)(2,1)}) %all-gather.4.cloned.1.call-update) | async-done | bytes 9437200 | tf_op jit(solution)/shard_map/all_gather | solution.py:22
  134.9 18.7 %all-to-all-done.2 = bf16[4,96,2048]{2,1,0:T(8,128)(2,1)S(1)} async-done(((bf16[4,96,2048]{2,1,0:T(8,128)(2,1)}), bf16[4,96,2048]{2,1,0:T(8,128)(2,1)S(1)}, u32[]{:S(2)}, u32[]{:S(2)}) %all-to-all-start.2) | async-done | bytes 1572896 | tf_op jit(solution)/shard_map/all_to_all | solution.py:38
  153.6 4.3 %fusion.4 = f32[384,768]{1,0:T(8,128)} fusion(bf16[384,2048]{1,0:T(8,128)(2,1)S(1)} %bitcast.31, bf16[2048,2304]{1,0:T(8,128)(2,1)} %all-gather.4.cloned.1.call-done), kind=kOutput, calls=%fused_computation.4 | convolution fusion | flops 1207959552 | bytes 5898240 | tf_op jit(solution)/shard_map/dot_general | solution.py:189
  157.9 7.4 %fusion.6 = bf16[384,2048]{1,0:T(8,128)(2,1)} fusion(bf16[2048,2304]{1,0:T(8,128)(2,1)} %all-gather.4.cloned.1.call-done, bf16[384,2048]{1,0:T(8,128)(2,1)S(1)} %bitcast.32, f32[384,768]{1,0:T(8,128)} %fusion.4), kind=kOutput, calls=%fused_computation.7 | convolution fusion | flops 2418475008 | bytes 10616832 | tf_op jit(solution)/shard_map/dot_general | solution.py:193
  165.3 23.8 %all_to_all.32 = bf16[4,96,2048]{2,1,0:T(8,128)(2,1)S(1)} all-to-all(bf16[4,96,2048]{2,1,0:T(8,128)(2,1)} %bitcast.33), channel_id=1, replica_groups=mesh['sp'=32,'tp'=4] {'tp'}, dimensions={0} | all-to-all | bytes 3145728 | tf_op jit(solution)/shard_map/all_to_all | solution.py:52
  189.1 0.3 convert_reduce_fusion
  189.4 0.0 copy-start.11
  189.4 0.3 fusion.27
  189.8 0.4 multiply_reduce_fusion
  190.1 0.0 copy-done.11
  190.2 1.2 multiply_convert_fusion
  (33 shorter events, 0.2 us)
Async XLA Ops:
  6.5 1.2 copy-start
  6.5 71.3 %all-gather.6.cloned.1.call-start = ((), (), s32[]{:S(2)}) async-start(), calls=%async_computation.5 | async-start | bytes 14598144 | tf_op jit(solution)/shard_map/all_gather | solution.py:161
  6.6 4.3 %copy-start.10 = (bf16[384,64]{0,1:T(8,128)(2,1)S(1)}, bf16[384,64]{0,1:T(8,128)(2,1)}, u32[]{:S(2)}) copy-start(bf16[384,64]{0,1:T(8,128)(2,1)} %param.17) | copy-start | bytes 147460
  9.2 3.0 %copy-start.6 = (bf16[768,64]{0,1:T(8,128)(2,1)S(1)}, bf16[768,64]{0,1:T(8,128)(2,1)}, u32[]{:S(2)}) copy-start(bf16[768,64]{0,1:T(8,128)(2,1)} %param.26) | copy-start | bytes 294916
  9.2 3.0 %copy-start.7 = (bf16[64,768]{1,0:T(8,128)(2,1)S(1)}, bf16[64,768]{1,0:T(8,128)(2,1)}, u32[]{:S(2)}) copy-start(bf16[64,768]{1,0:T(8,128)(2,1)} %param.25) | copy-start | bytes 294916
  9.2 3.0 %copy-start.8 = (bf16[64,768]{1,0:T(8,128)(2,1)S(1)}, bf16[64,768]{1,0:T(8,128)(2,1)}, u32[]{:S(2)}) copy-start(bf16[64,768]{1,0:T(8,128)(2,1)} %param.24) | copy-start | bytes 294916
  10.7 2.3 %copy-start.1 = (bf16[256,2048]{1,0:T(8,128)(2,1)S(1)}, bf16[256,2048]{1,0:T(8,128)(2,1)}, u32[]{:S(2)}) copy-start(bf16[256,2048]{1,0:T(8,128)(2,1)} %param.21) | copy-start | bytes 3145732
  11.4 0.8 copy-start.2
  12.2 122.7 %all-gather.4.cloned.1.call-start = ((), (), s32[]{:S(2)}) async-start(), calls=%async_computation.4 | async-start | bytes 9732096 | tf_op jit(solution)/shard_map/all_gather | solution.py:22
  15.6 5.0 %copy-start.9 = (bf16[384,2,64]{0,2,1:T(8,128)(2,1)S(1)}, bf16[384,2,64]{0,2,1:T(8,128)(2,1)}, u32[]{:S(2)}) copy-start(bf16[384,2,64]{0,2,1:T(8,128)(2,1)} %param.15) | copy-start | bytes 294916
  15.6 5.4 %copy-start.4 = (bf16[384,2,128]{2,1,0:T(2,128)(2,1)S(1)}, bf16[384,2,128]{2,1,0:T(2,128)(2,1)}, u32[]{:S(2)}) copy-start(bf16[384,2,128]{2,1,0:T(2,128)(2,1)} %param.14) | copy-start | bytes 589828
  15.6 96.8 %all-to-all-start.1 = ((bf16[4,256,2048]{2,1,0:T(8,128)(2,1)}), bf16[4,256,2048]{2,1,0:T(8,128)(2,1)}, u32[]{:S(2)}, u32[]{:S(2)}) async-start(bf16[4,256,2048]{2,1,0:T(8,128)(2,1)} %broadcast_in_dim.7), calls=%async_computation.1 | async-start | bytes 8388608 | tf_op jit(solution)/shard_map/all_to_all | solution.py:38
  77.8 46.0 %copy-start.3 = (bf16[96,2048]{1,0:T(8,128)(2,1)S(1)}, bf16[96,2048]{1,0:T(8,128)(2,1)}, u32[]{:S(2)}) copy-start(bf16[96,2048]{1,0:T(8,128)(2,1)} %param.22) | copy-start | bytes 1179652
  123.8 3.6 %copy-start.5 = (f32[2048]{0:T(1024)S(1)}, f32[2048]{0:T(1024)}, u32[]{:S(2)}) copy-start(f32[2048]{0:T(1024)} %param.23) | copy-start | bytes 24580
  129.0 24.7 %all-to-all-start.2 = ((bf16[4,96,2048]{2,1,0:T(8,128)(2,1)}), bf16[4,96,2048]{2,1,0:T(8,128)(2,1)S(1)}, u32[]{:S(2)}, u32[]{:S(2)}) async-start(bf16[4,96,2048]{2,1,0:T(8,128)(2,1)} %broadcast_in_dim.8), calls=%async_computation.2 | async-start | bytes 3145728 | tf_op jit(solution)/shard_map/all_to_all | solution.py:38
  189.4 0.8 copy-start.11
Sparse Core Ops, SparseCore 0:
  12.3 65.4 all-gather.5
  80.1 54.7 all-gather.3

commit v2 on v1

v2 whole, which is shorter than its diff:
```python
import functools
import math

import jax
import jax.numpy as jnp
from jax import lax
from jax.experimental import pallas as pl
from jax.experimental.pallas import tpu as pltpu
from jax.sharding import PartitionSpec as P

theta_base = 10000.0
residual_weight = 8.0**0.25
norm_floor = 1.0
big_negative = -1e30
F32 = jnp.float32
BF16 = jnp.bfloat16


def rotate(vector, first_row):
    half = vector.shape[-1] // 2
    rates = theta_base ** (-2.0 * jnp.arange(half, dtype=jnp.float32) / vector.shape[-1])
    places = (first_row + jnp.arange(vector.shape[0], dtype=jnp.int32)).astype(jnp.float32)
    angle = places[:, None] * rates[None, :]
    angle = angle.reshape((vector.shape[0],) + (1,) * (vector.ndim - 2) + (half,))
    cosine = jnp.cos(angle)
    sine = jnp.sin(angle)
    left = vector[..., :half]
    right = vector[..., half:]
    return jnp.concatenate([left * cosine - right * sine, left * sine + right * cosine], axis=-1)


def latent_norm(latent, latent_gain):
    wide = latent.astype(jnp.float32)
    factor = lax.rsqrt(jnp.mean(wide * wide, axis=-1, keepdims=True) + norm_floor)
    return (wide * factor * latent_gain).astype(jnp.bfloat16)


def layer_norm(values, gain):
    centre = jnp.mean(values, axis=-1, keepdims=True)
    centred = values - centre
    spread = jnp.mean(centred * centred, axis=-1, keepdims=True)
    return centred * lax.rsqrt(spread + norm_floor) * gain


def attend_chunk(kv, q_ref, m_ref, l_ref, acc_ref, rows, const, diag):
    half = rows // 2
    blocks = rows // 128
    r = kv[4 * rows : 4 * rows + half, :]
    for h in range(2):
        top = jnp.concatenate([kv[h * rows : h * rows + half, :], r], axis=1)
        low = jnp.concatenate([kv[h * rows + half : (h + 1) * rows, :], r], axis=1)
        s = jnp.concatenate(
            [
                jnp.dot(top, q_ref[2 * h], preferred_element_type=F32),
                jnp.dot(low, q_ref[2 * h + 1], preferred_element_type=F32),
            ],
            axis=0,
        )
        s = s * const
        if diag:
            key = lax.broadcasted_iota(jnp.int32, s.shape, 0)
            query = lax.broadcasted_iota(jnp.int32, s.shape, 1)
            s = jnp.where(key <= query, s, big_negative)
        m_old = m_ref[h]
        m_new = jnp.maximum(m_old, jnp.max(s, axis=0, keepdims=True))
        p = jnp.exp2(s - m_new)
        alpha = jnp.exp2(m_old - m_new)
        l_ref[h] = l_ref[h] * alpha + jnp.sum(p, axis=0, keepdims=True)
        m_ref[h] = m_new
        at = 2 * rows + h * rows
        vt = jnp.concatenate([kv[at + 128 * i : at + 128 * (i + 1), :] for i in range(blocks)], axis=1)
        acc_ref[h] = acc_ref[h] * alpha + jnp.dot(vt, p.astype(BF16), preferred_element_type=F32)


MESH = pl.DeviceIdType.MESH
ITEMS = (
    (0, 0), (-1, 0), (1, 0), (0, -1), (0, 1), (2, 0), (-1, -1), (-1, 1),
    (1, -1), (1, 1), (0, 2), (2, -1), (2, 1), (-1, 2), (1, 2), (2, 2),
)
PLACE = {item: k for k, item in enumerate(ITEMS)}
STEPS = 2 * len(ITEMS)


def remote(src, dst, send_sem, recv_sem, device):
    return pltpu.make_async_remote_copy(
        src_ref=src, dst_ref=dst, send_sem=send_sem, recv_sem=recv_sem, device_id=device, device_id_type=MESH
    )


class Torus:
    def __init__(self):
        self.me = lax.axis_index("sp")
        self.x = lax.axis_index("tp")
        self.c = lax.rem(self.me, 2)
        chip = self.me // 2
        z, y = chip // 4, lax.rem(chip, 4)
        self.a = z + self.c * (y - z)
        self.b = y + self.c * (z - y)
        self.step_a = 8 - 6 * self.c
        self.step_b = 2 + 6 * self.c

    def index(self, da, db):
        at_a = lax.rem(self.a + da + 4, 4)
        at_b = lax.rem(self.b + db + 4, 4)
        return at_a * self.step_a + at_b * self.step_b + self.c

    def twin_index(self, da, db):
        at_b = lax.rem(self.b + da + 4, 4)
        at_a = lax.rem(self.a + db + 4, 4)
        return at_a * self.step_a + at_b * self.step_b + 1 - self.c

    def at(self, da, db):
        return (self.index(da, db), self.x)

    def twin(self):
        return (self.me + 1 - 2 * self.c, self.x)

    def along_x(self, d):
        return (self.me, lax.rem(self.x + d + 4, 4))


class Gather:
    def __init__(self, torus, buf, send_sems, recv_sems, twin_sems):
        self.torus, self.buf = torus, buf
        self.send_sems, self.recv_sems, self.twin_sems = send_sems, recv_sems, twin_sems
        self.half = buf.shape[1] // 2

    def part(self, slot, which):
        if which is None:
            return self.buf.at[slot]
        return self.buf.at[slot, pl.ds(which * self.half, self.half)]

    def copies(self, k):
        t = self.torus
        da, db = ITEMS[k]
        slot = t.index(da, db)
        plan = []
        if db == 0:
            if da == 0:
                plan += [(2, (1, 0), (-1, 0), None), (3, (-1, 0), (1, 0), None)]
            plan += [(0, (0, 1), (da, -1), None), (1, (0, -1), (da, 1), None)]
            if da == -1:
                plan += [(2, (1, 0), (2, 0), 0)]
            if da == 1:
                plan += [(2, (-1, 0), (2, 0), 1)]
        if db == -1:
            plan += [(0, (0, 1), (da, 2), 0)]
        if db == 1:
            plan += [(1, (0, -1), (da, 2), 1)]
        out = []
        for sem, to, name, which in plan:
            ref = self.part(slot, which)
            recv = self.recv_sems.at[PLACE[name], which or 0]
            out.append(remote(ref, ref, self.send_sems.at[k, sem], recv, t.at(*to)))
        ref = self.part(slot, None)
        out.append(remote(ref, ref, self.send_sems.at[k, 4], self.twin_sems.at[k], t.twin()))
        return out

    def send(self, k):
        for copy in self.copies(k):
            copy.start()

    def sent(self):
        for k in range(len(ITEMS)):
            for copy in self.copies(k):
                copy.wait_send()

    def arrived(self, k):
        t = self.torus
        da, db = ITEMS[k]
        slot = t.index(da, db)
        for which in (0, 1) if 2 in (da, db) and not (da == 2 and db in (-1, 1)) else (None,):
            ref = self.part(slot, which)
            remote(ref, ref, self.send_sems.at[k, 0], self.recv_sems.at[k, which or 0], t.twin()).wait_recv()

    def twin_arrived(self, k, slot):
        ref = self.part(slot, None)
        remote(ref, ref, self.send_sems.at[0, 0], self.twin_sems.at[k], self.torus.twin()).wait_recv()


def whole_kernel(
    rows,
    const,
    slab_hbm,
    weights_hbm,
    proj_hbm,
    q_ref,
    stream_ref,
    mix_gain_ref,
    mlp_gain_ref,
    out_ref,
    kv,
    weights,
    proj,
    m_ref,
    l_ref,
    acc_ref,
    attended,
    row_heads,
    sums,
    mixed,
    hidden,
    far_out,
    plus_out,
    minus_out,
    far_plus,
    far_minus,
    from_plus,
    from_minus,
    load_sems,
    kv_send,
    kv_recv,
    kv_twin,
    w_send,
    w_recv,
    w_twin,
    proj_send,
    proj_recv,
    x_send,
    x_recv,
):
    t = Torus()
    me, x = t.me, t.x
    loads = [
        pltpu.make_async_copy(slab_hbm, kv.at[me], load_sems.at[0]),
        pltpu.make_async_copy(proj_hbm, proj.at[x], load_sems.at[1]),
        pltpu.make_async_copy(weights_hbm, weights.at[me], load_sems.at[2]),
    ]
    for load in loads:
        load.start()

    plus, minus, across = t.along_x(1), t.along_x(-1), t.along_x(2)
    peers = (t.at(1, 0), t.at(-1, 0), t.at(0, 1), t.at(0, -1), t.twin(), plus, minus, across)
    barrier = pltpu.get_barrier_semaphore()
    for peer in peers:
        pl.semaphore_signal(barrier, inc=1, device_id=peer, device_id_type=MESH)
    pl.semaphore_wait(barrier, len(peers))

    pieces = Gather(t, kv, kv_send, kv_recv, kv_twin)
    halves = Gather(t, weights, w_send, w_recv, w_twin)

    share = proj.shape[1] // 2

    def proj_part(d, which):
        slot = lax.rem(x + d + 4, 4)
        size = share if which is None else share // 2
        first = t.c * share + (0 if which is None else which * size)
        return proj.at[slot, pl.ds(pl.multiple_of(first, size), size)]

    def proj_copy(d, which, sem, recv, to):
        ref = proj_part(d, which)
        return remote(ref, ref, proj_send.at[sem], proj_recv.at[recv], to)

    proj_first = [proj_copy(0, None, 0, 0, plus), proj_copy(0, None, 1, 1, minus)]
    proj_second = [
        proj_copy(-1, 0, 2, 2, plus),
        proj_copy(1, 1, 3, 3, minus),
        proj_copy(-1, None, 4, 4, t.twin()),
        proj_copy(1, None, 5, 5, t.twin()),
    ]
    proj_third = [proj_copy(2, None, 6, 6, t.twin())]

    def twin_proj(d, recv):
        slot = lax.rem(x + d + 4, 4)
        first = (1 - t.c) * share
        ref = proj.at[slot, pl.ds(pl.multiple_of(first, share), share)]
        return remote(ref, ref, proj_send.at[0], proj_recv.at[recv], t.twin())

    loads[0].wait()
    pieces.send(0)
    loads[1].wait()
    for copy in proj_first:
        copy.start()

    m_ref[...] = jnp.full_like(m_ref, big_negative)
    l_ref[...] = jnp.zeros_like(l_ref)
    acc_ref[...] = jnp.zeros_like(acc_ref)
    attend_chunk(kv.at[me], q_ref, m_ref, l_ref, acc_ref, rows, const, True)
    loads[2].wait()

    def step(i, carry):
        item = i // 2
        odd = lax.rem(i, 2)
        for k in range(1, len(ITEMS)):

            @pl.when(i == 2 * (k - 1))
            def _():
                pieces.arrived(k)
                pieces.send(k)

        @pl.when(i == PROJ_SECOND)
        def _():
            proj_copy(-1, None, 0, 0, minus).wait_recv()
            proj_copy(1, None, 0, 1, minus).wait_recv()
            for copy in proj_second:
                copy.start()

        @pl.when(i == PROJ_THIRD)
        def _():
            proj_copy(2, 0, 0, 2, minus).wait_recv()
            proj_copy(2, 1, 0, 3, minus).wait_recv()
            for copy in proj_third:
                copy.start()

        @pl.when(i == WEIGHTS_FIRST)
        def _():
            halves.send(0)

        da, db = jnp.int32(0), jnp.int32(0)
        number = item + 1 - odd
        for k, (ka, kb) in enumerate(ITEMS):
            da = jnp.where(number == k, ka, da)
            db = jnp.where(number == k, kb, db)
        off_a = jnp.where(odd == 1, db, da)
        off_b = jnp.where(odd == 1, da, db)
        at_a = lax.rem(t.a + off_a + 4, 4)
        at_b = lax.rem(t.b + off_b + 4, 4)
        slot = at_a * t.step_a + at_b * t.step_b + jnp.where(odd == 1, 1 - t.c, t.c)

        @pl.when(odd == 1)
        def _():
            pieces.twin_arrived(item, slot)

        @pl.when(jnp.logical_and(slot < me, i != STEPS - 2))
        def _():
            attend_chunk(kv.at[slot], q_ref, m_ref, l_ref, acc_ref, rows, const, False)

        return carry

    lax.fori_loop(0, STEPS, step, 0)

    for h in range(2):
        attended[:, 128 * h : 128 * (h + 1)] = (acc_ref[h] / l_ref[h]).T.astype(BF16)
    own = rows // 4

    def own_rows(d):
        first = lax.rem(x + d + 4, 4) * own
        return attended.at[pl.ds(pl.multiple_of(first, own), own)]

    heads_out = [
        remote(own_rows(2), row_heads.at[x], x_send.at[0], x_recv.at[0], across),
        remote(own_rows(1), row_heads.at[x], x_send.at[1], x_recv.at[1], plus),
        remote(own_rows(-1), row_heads.at[x], x_send.at[2], x_recv.at[2], minus),
    ]
    for copy in heads_out:
        copy.start()
    row_heads[x] = attended[pl.ds(pl.multiple_of(x * own, own), own), :]

    def weights_step(first, last):
        for k in range(first, last):
            halves.arrived(k)
            halves.send(k)

    weights_step(1, 3)
    for d, sem in ((1, 4), (-1, 5), (2, 6)):
        twin_proj(d, sem).wait_recv()
    for d, sem in ((2, 0), (-1, 1), (1, 2)):
        ref = row_heads.at[lax.rem(x + d + 4, 4)]
        remote(ref, ref, x_send.at[0], x_recv.at[sem], plus).wait_recv()

    lhs = jnp.concatenate([row_heads[p] for p in range(4)], axis=1)
    width = sums.shape[1]

    def project(n, carry):
        cols = pl.ds(pl.multiple_of(n * 256, 256), 256)
        rhs = proj[:, :, cols].reshape(4 * proj.shape[1], 256)
        sums[pl.ds(0, own), cols] = jnp.dot(lhs, rhs, preferred_element_type=F32)
        return carry

    lax.fori_loop(0, width // 256, project, 0)
    mixed[x] = layer_norm(
        residual_weight * stream_ref[...].astype(F32) + sums[pl.ds(0, own), :], mix_gain_ref[...]
    ).astype(BF16)

    half = own // 2

    def mixed_copy(d, which, sem, recv, to):
        slot = lax.rem(x + d + 4, 4)
        ref = mixed.at[slot] if which is None else mixed.at[slot, pl.ds(which * half, half)]
        return remote(ref, ref, x_send.at[sem], x_recv.at[recv], to)

    mixed_first = [mixed_copy(0, None, 3, 3, plus), mixed_copy(0, None, 4, 4, minus)]
    mixed_second = [mixed_copy(-1, 0, 5, 5, plus), mixed_copy(1, 1, 6, 6, minus)]
    for copy in mixed_first:
        copy.start()
    weights_step(3, 10)
    mixed_copy(-1, None, 3, 3, plus).wait_recv()
    mixed_copy(1, None, 3, 4, plus).wait_recv()
    for copy in mixed_second:
        copy.start()
    weights_step(10, 13)
    mixed_copy(2, 0, 3, 5, plus).wait_recv()
    mixed_copy(2, 1, 3, 6, plus).wait_recv()
    weights_step(13, 16)
    for k, item in enumerate(ITEMS):
        halves.twin_arrived(k, t.twin_index(*item))

    count = weights.shape[0]
    depth = weights.shape[1] // 3
    units = weights.shape[2]

    def feed(first, second):
        into = jnp.concatenate(
            [mixed[lax.rem(x + first + 4, 4)], mixed[lax.rem(x + second + 4, 4)]], axis=0
        )

        def expand(n, carry):
            cols = pl.ds(pl.multiple_of(n * 256, 256), 256)
            gate = jnp.dot(
                into, weights[:, 0:depth, cols].reshape(count * depth, 256), preferred_element_type=F32
            )
            up = jnp.dot(
                into, weights[:, depth : 2 * depth, cols].reshape(count * depth, 256), preferred_element_type=F32
            )
            hidden[:, cols] = (gate / (1.0 + jnp.exp(-gate)) * up).astype(BF16)
            return carry

        lax.fori_loop(0, units // 256, expand, 0)
        group = 256 // depth

        def lower(n, carry):
            rhs = weights[pl.ds(n * group, group), 2 * depth : 3 * depth, :].reshape(256, units)
            sums[:, pl.ds(pl.multiple_of(n * 256, 256), 256)] = lax.dot_general(
                hidden[...], rhs, (((1,), (1,)), ((), ())), preferred_element_type=F32
            )
            return carry

        lax.fori_loop(0, count // group, lower, 0)

    top, low = pl.ds(0, half), pl.ds(half, half)

    def result_copy(src, src_rows, dst, dst_rows, sem, to):
        s = src.at[src_rows]
        d = dst if dst_rows is None else dst.at[dst_rows]
        return remote(s, d, x_send.at[sem], x_recv.at[sem], to)

    feed(2, 1)
    far_out[...] = sums[0:own, :].astype(BF16)
    plus_out[...] = sums[own : 2 * own, :].astype(BF16)
    back = [
        result_copy(far_out, top, far_minus, None, 7, plus),
        result_copy(far_out, low, far_plus, None, 8, minus),
        result_copy(plus_out, low, from_minus, low, 9, plus),
        result_copy(minus_out, top, from_plus, top, 10, minus),
        result_copy(plus_out, top, from_minus, top, 11, plus),
        result_copy(minus_out, low, from_plus, low, 12, minus),
    ]
    for copy in back[:3]:
        copy.start()
    feed(-1, 0)
    minus_out[...] = sums[0:own, :].astype(BF16)
    back[3].start()
    back[0].wait_recv()
    plus_out[top, :] = (plus_out[top, :].astype(F32) + far_minus[...].astype(F32)).astype(BF16)
    back[4].start()
    back[1].wait_recv()
    minus_out[low, :] = (minus_out[low, :].astype(F32) + far_plus[...].astype(F32)).astype(BF16)
    back[5].start()
    for copy in back[2:]:
        copy.wait_recv()
    lowered = sums[own : 2 * own, :] + from_plus[...].astype(F32) + from_minus[...].astype(F32)
    out_ref[...] = layer_norm(
        residual_weight * mixed[x].astype(F32) + 0.5 * lowered, mlp_gain_ref[...]
    ).astype(BF16)

    pieces.sent()
    halves.sent()
    for copy in proj_first + proj_second + proj_third + heads_out + mixed_first + mixed_second + back:
        copy.wait_send()


PROJ_SECOND = 11
PROJ_THIRD = 19
WEIGHTS_FIRST = 23


def per_device(
    queries_nope,
    queries_rope,
    latent,
    rope_key,
    latent_gain,
    key_up,
    value_up,
    out_proj,
    stream,
    mix_gain,
    w_gate,
    w_up,
    w_down,
    mlp_gain,
):
    rows, heads, head_dim = queries_nope.shape
    rope_dim = queries_rope.shape[2]
    count = lax.axis_size("sp")
    tp = lax.axis_size("tp")
    own, width = stream.shape
    units = w_gate.shape[1]
    first_row = lax.axis_index("sp") * rows
    query_turned = rotate(queries_rope.astype(F32), first_row).astype(BF16)
    key_turned = rotate(rope_key.astype(F32), first_row).astype(BF16)
    normed = latent_norm(latent, latent_gain)
    keys = jnp.dot(normed, key_up, preferred_element_type=F32).astype(BF16)
    values_t = lax.dot_general(
        value_up, normed, (((0,), (1,)), ((), ())), preferred_element_type=F32
    ).astype(BF16)
    half = rows // 2
    slab = jnp.concatenate(
        [keys[:, :128], keys[:, 128:]]
        + [values_t[128 * h : 128 * (h + 1), 128 * i : 128 * (i + 1)] for h in range(2) for i in range(rows // 128)]
        + [jnp.concatenate([key_turned[:half], key_turned[half:]], axis=1)],
        axis=0,
    )
    weights = jnp.concatenate([w_gate, w_up, w_down.T], axis=0)
    qn = jnp.transpose(queries_nope, (1, 2, 0))
    qr = jnp.transpose(query_turned, (1, 2, 0))
    zero = jnp.zeros_like(qr)
    q_all = jnp.stack(
        [jnp.concatenate([qn, qr, zero], axis=1), jnp.concatenate([qn, zero, qr], axis=1)], axis=1
    ).reshape(2 * heads, 2 * head_dim, rows)
    const = (head_dim + rope_dim) ** (-0.5) * math.log2(math.e)
    vmem = pl.BlockSpec(memory_space=pltpu.VMEM)
    hbm = pl.BlockSpec(memory_space=pl.ANY)
    dma = pltpu.SemaphoreType.DMA
    return pl.pallas_call(
        functools.partial(whole_kernel, rows, const),
        out_shape=jax.ShapeDtypeStruct((own, width), BF16),
        in_specs=[hbm, hbm, hbm, vmem, vmem, vmem, vmem],
        out_specs=vmem,
        scratch_shapes=[
            pltpu.VMEM((count, *slab.shape), BF16),
            pltpu.VMEM((count, *weights.shape), BF16),
            pltpu.VMEM((tp, *out_proj.shape), BF16),
            pltpu.VMEM((2, 1, rows), F32),
            pltpu.VMEM((2, 1, rows), F32),
            pltpu.VMEM((2, 128, rows), F32),
            pltpu.VMEM((rows, heads * head_dim), BF16),
            pltpu.VMEM((tp, own, heads * head_dim), BF16),
            pltpu.VMEM((2 * own, width), F32),
            pltpu.VMEM((tp, own, width), BF16),
            pltpu.VMEM((2 * own, units), BF16),
            pltpu.VMEM((own, width), BF16),
            pltpu.VMEM((own, width), BF16),
            pltpu.VMEM((own, width), BF16),
            pltpu.VMEM((own // 2, width), BF16),
            pltpu.VMEM((own // 2, width), BF16),
            pltpu.VMEM((own, width), BF16),
            pltpu.VMEM((own, width), BF16),
            dma((3,)),
            dma((16, 5)),
            dma((16, 2)),
            dma((16,)),
            dma((16, 5)),
            dma((16, 2)),
            dma((16,)),
            dma((7,)),
            dma((7,)),
            dma((13,)),
            dma((13,)),
        ],
        compiler_params=pltpu.CompilerParams(
            collective_id=0, has_side_effects=True, vmem_limit_bytes=60 * 1024 * 1024
        ),
        name="layer",
    )(slab, weights, out_proj, q_all, stream, mix_gain.reshape(1, -1), mlp_gain.reshape(1, -1))


def solution(mesh):
    return jax.shard_map(
        per_device,
        mesh=mesh,
        in_specs=(
            P("sp", "tp", None),
            P("sp", "tp", None),
            P("sp", None),
            P("sp", None),
            P(),
            P(None, "tp"),
            P(None, "tp"),
            P("tp", None),
            P(("sp", "tp"), None),
            P(),
            P("sp", "tp"),
            P("sp", "tp"),
            P("tp", "sp"),
            P(),
        ),
        out_specs=P(("sp", "tp"), None),
        check_vma=False,
    )
```

time: 199 us -> 117 us (0.59)
  the two profiles are of different devices: /device:TPU:120 before, /device:TPU:1 now
where the time goes in v2:
time: 117 us; the launch traced here: 116 us
  Pallas kernels  101 us (86%)
  local copies, waits for them, and re-layouts  7.76 us (7%)
  other arithmetic  5.5 us (5%)
    pallas_call x1, Pallas kernels, per_device(): pl.pallas_call(functools.partial(whole_kernel, rows, const), out_shape=ja...  101 us
    unnamed x32, local copies, waits for them, and re-layouts  5.43 us
    another operation x2, other arithmetic, per_device(): jnp.stack([jnp.concatenate([qn, qr, zero], axis=1), jnp.concatenate([qn,...  2.41 us

profile of v2, /device:TPU:1, one launch (start us, length us, event | category | flops | bytes accessed | tf_op | source)
XLA Modules:
  0.0 115.6 jit_solution(10370729359847051969)
XLA Ops:
  0.0 0.0 copy-start
  0.0 0.0 copy-start.2
  0.0 1.2 %fusion.1 = f32[384]{0:T(512)S(1)} fusion(bf16[384,512]{1,0:T(8,128)(2,1)} %param.16), kind=kLoop, calls=%fused_computation.5 | loop fusion | flops 589440 | bytes 394752 | tf_op jit(solution)/shard_map/reduce_sum | solution.py:34
  1.2 0.0 copy-start.10
  1.2 0.0 copy-done
  1.3 0.0 copy-done.2
  1.3 0.6 copy-done.10
  1.9 0.0 copy-start.9
  1.9 0.4 fusion
  2.4 0.5 copy-done.9
  2.9 0.3 convolution_convert_fusion.1
  3.3 0.0 copy-start.8
  3.3 0.8 copy-done.8
  4.1 0.1 copy.21
  4.3 0.8 multiply_cosine_fusion
  5.1 0.1 fusion.6
  5.2 0.1 fusion.8.slab_hbm
  5.3 0.0 copy-start.1
  5.3 0.1 copy.23
  5.4 0.0 copy-start.7
  5.4 0.1 copy.24
  5.5 0.9 copy-done.7
  6.5 0.0 copy-done.1
  6.5 0.0 copy-start.3
  6.5 0.2 copy.25
  6.7 0.1 broadcast_in_dim.2
  6.8 0.6 copy-done.3
  7.4 1.3 %maximum_bitcast_fusion = (bf16[2,1,256,384]{2,0,3,1:T(2,128)(2,1)S(1)}, bf16[2,1,256,384]{2,0,3,1:T(2,128)(2,1)S(1)}) fusion(bf16[2,64,384]{1,0,2:T(2,128)(2,1)S(1)} %broadcast_in_dim.2, bf16[2,64,384]{1,0,2:T(2,128)(2,1)S(1)} %copy.25, bf16[2,128,384]{1,0,2:T(2,128)(2,1)S(1)} %bitcast.16), kind=kLoop, calls=%fused_computation.9 | loop fusion | flops 2162688 | bytes 1179648 | tf_op jit(solution)/shard_map/stack | solution.py:518
  8.7 1.1 pad_maximum_fusion
  9.8 0.0 copy-start.4
  9.9 0.0 copy-start.5
  9.9 0.0 copy-start.6
  9.9 1.8 %copy.27 = bf16[2,2,256,384]{3,2,1,0:T(8,128)(2,1)} copy(bf16[2,2,256,384]{2,0,3,1:T(2,128)(2,1)S(1)} %pad_maximum_fusion) | data formatting | bytes 1572864 | tf_op jit(solution)/shard_map/stack | solution.py:518
  11.7 0.0 copy-done.4
  11.7 0.0 copy-done.5
  11.7 0.0 copy-done.6
  11.7 0.7 pad_maximum_fusion.1.weights_hbm
  12.5 101.4 %layer.1 = bf16[96,2048]{1,0:T(8,128)(2,1)} custom-call(bf16[1728,128]{1,0:T(8,128)(2,1)} %copy-done.1, bf16[192,768]{1,0:T(8,128)(2,1)} %pad_maximum_fusion.1.weights_hbm, bf16[256,2048]{1,0:T(8,128)(2,1)} %proj_hbm.1, bf16[4,256,384]{2,1,0:T(8,128)(2,1)} %bitcast.15, bf16[96,2048]{1,0:T(8,128)(2,1)} %stream_ref.1, f32[1,2048]{1,0:T(1,128)} %bitcast.18, ...), custom_call_target="tpu_custom_call" | custom-call | tf_op jit(solution)/shard_map/layer/pallas_call | solution.py:525
  113.9 1.8 %copy.37 = bf16[96,2048]{1,0:T(8,128)(2,1)} copy(bf16[96,2048]{1,0:T(8,128)(2,1)} %layer.1) | data formatting | bytes 786432
  (15 shorter events, 0.2 us)
Async XLA Ops:
  0.0 1.2 %copy-start = (bf16[512,256]{1,0:T(8,128)(2,1)S(1)}, bf16[512,256]{1,0:T(8,128)(2,1)}, u32[]{:S(2)}) copy-start(bf16[512,256]{1,0:T(8,128)(2,1)} %param.20) | copy-start | bytes 786436
  0.0 1.3 %copy-start.2 = (bf16[384,512]{1,0:T(8,128)(2,1)S(1)}, bf16[384,512]{1,0:T(8,128)(2,1)}, u32[]{:S(2)}) copy-start(bf16[384,512]{1,0:T(8,128)(2,1)} %param.16) | copy-start | bytes 1179652
  1.2 0.7 copy-start.10
  1.9 0.9 copy-start.9
  3.3 0.8 copy-start.8
  5.3 1.1 copy-start.1
  5.4 1.0 copy-start.7
  6.5 0.9 copy-start.3
  9.8 1.9 %copy-start.4 = (bf16[768,64]{0,1:T(8,128)(2,1)S(1)}, bf16[768,64]{0,1:T(8,128)(2,1)}, u32[]{:S(2)}) copy-start(bf16[768,64]{0,1:T(8,128)(2,1)} %param.26) | copy-start | bytes 294916
  9.9 1.9 %copy-start.5 = (bf16[64,768]{1,0:T(8,128)(2,1)S(1)}, bf16[64,768]{1,0:T(8,128)(2,1)}, u32[]{:S(2)}) copy-start(bf16[64,768]{1,0:T(8,128)(2,1)} %param.25) | copy-start | bytes 294916
  9.9 1.9 %copy-start.6 = (bf16[64,768]{1,0:T(8,128)(2,1)S(1)}, bf16[64,768]{1,0:T(8,128)(2,1)}, u32[]{:S(2)}) copy-start(bf16[64,768]{1,0:T(8,128)(2,1)} %param.24) | copy-start | bytes 294916

commit v3 on v2

--- a/solution.py
+++ b/solution.py
@@ -3,6 +3,7 @@
 
 import jax
 import jax.numpy as jnp
+import numpy as np
 from jax import lax
 from jax.experimental import pallas as pl
 from jax.experimental.pallas import tpu as pltpu
@@ -16,23 +17,18 @@
 BF16 = jnp.bfloat16
 
 
-def rotate(vector, first_row):
-    half = vector.shape[-1] // 2
-    rates = theta_base ** (-2.0 * jnp.arange(half, dtype=jnp.float32) / vector.shape[-1])
-    places = (first_row + jnp.arange(vector.shape[0], dtype=jnp.int32)).astype(jnp.float32)
-    angle = places[:, None] * rates[None, :]
-    angle = angle.reshape((vector.shape[0],) + (1,) * (vector.ndim - 2) + (half,))
-    cosine = jnp.cos(angle)
-    sine = jnp.sin(angle)
-    left = vector[..., :half]
-    right = vector[..., half:]
-    return jnp.concatenate([left * cosine - right * sine, left * sine + right * cosine], axis=-1)
-
-
-def latent_norm(latent, latent_gain):
-    wide = latent.astype(jnp.float32)
-    factor = lax.rsqrt(jnp.mean(wide * wide, axis=-1, keepdims=True) + norm_floor)
-    return (wide * factor * latent_gain).astype(jnp.bfloat16)
+def turn_tables(rows, count, rope_dim):
+    rates = theta_base ** (-2.0 * np.arange(rope_dim // 2) / rope_dim)[:, None]
+    inner = rates * np.arange(rows)
+    outer = (rates * (np.arange(count) * rows)).T[:, :, None] + np.zeros((1, 1, 128))
+    pair = lambda angle: jnp.asarray(np.stack([np.cos(angle), np.sin(angle)]), F32)
+    return pair(inner), jnp.moveaxis(pair(outer), 0, 1)
+
+
+def turn(v, cosine, sine):
+    half = v.shape[0] // 2
+    a, b = v[:half], v[half:]
+    return jnp.concatenate([a * cosine - b * sine, a * sine + b * cosine], axis=0)
 
 
 def layer_norm(values, gain):
@@ -42,21 +38,26 @@
     return centred * lax.rsqrt(spread + norm_floor) * gain
 
 
-def attend_chunk(kv, q_ref, m_ref, l_ref, acc_ref, rows, const, diag):
+def scores(kv, h, q_ref, rows, const):
     half = rows // 2
-    blocks = rows // 128
     r = kv[4 * rows : 4 * rows + half, :]
+    top = jnp.concatenate([kv[h * rows : h * rows + half, :], r], axis=1)
+    low = jnp.concatenate([kv[h * rows + half : (h + 1) * rows, :], r], axis=1)
+    both = [
+        jnp.dot(top, q_ref[2 * h], preferred_element_type=F32),
+        jnp.dot(low, q_ref[2 * h + 1], preferred_element_type=F32),
+    ]
+    return jnp.concatenate(both, axis=0) * const
+
+
+def values_of(kv, h, rows):
+    at = 2 * rows + h * rows
+    return [kv[at + 128 * i : at + 128 * (i + 1), :] for i in range(rows // 128)]
+
+
+def attend(pieces, q_ref, m_ref, l_ref, acc_ref, rows, const, diag=False):
     for h in range(2):
-        top = jnp.concatenate([kv[h * rows : h * rows + half, :], r], axis=1)
-        low = jnp.concatenate([kv[h * rows + half : (h + 1) * rows, :], r], axis=1)
-        s = jnp.concatenate(
-            [
-                jnp.dot(top, q_ref[2 * h], preferred_element_type=F32),
-                jnp.dot(low, q_ref[2 * h + 1], preferred_element_type=F32),
-            ],
-            axis=0,
-        )
-        s = s * const
+        s = jnp.concatenate([scores(kv, h, q_ref, rows, const) for kv in pieces], axis=0)
         if diag:
             key = lax.broadcasted_iota(jnp.int32, s.shape, 0)
             query = lax.broadcasted_iota(jnp.int32, s.shape, 1)
@@ -67,8 +68,7 @@
         alpha = jnp.exp2(m_old - m_new)
         l_ref[h] = l_ref[h] * alpha + jnp.sum(p, axis=0, keepdims=True)
         m_ref[h] = m_new
-        at = 2 * rows + h * rows
-        vt = jnp.concatenate([kv[at + 128 * i : at + 128 * (i + 1), :] for i in range(blocks)], axis=1)
+        vt = jnp.concatenate([block for kv in pieces for block in values_of(kv, h, rows)], axis=1)
         acc_ref[h] = acc_ref[h] * alpha + jnp.dot(vt, p.astype(BF16), preferred_element_type=F32)
 
 
@@ -78,7 +78,6 @@
     (1, -1), (1, 1), (0, 2), (2, -1), (2, 1), (-1, 2), (1, 2), (2, 2),
 )
 PLACE = {item: k for k, item in enumerate(ITEMS)}
-STEPS = 2 * len(ITEMS)
 
 
 def remote(src, dst, send_sem, recv_sem, device):
@@ -181,14 +180,33 @@
 def whole_kernel(
     rows,
     const,
-    slab_hbm,
-    weights_hbm,
+    latent_hbm,
+    rope_key_hbm,
+    key_up_hbm,
+    value_up_hbm,
+    inner_hbm,
+    qn_hbm,
+    qr_hbm,
     proj_hbm,
-    q_ref,
-    stream_ref,
+    gate_hbm,
+    up_hbm,
+    down_hbm,
+    stream_hbm,
+    outer_hbm,
+    latent_gain_ref,
     mix_gain_ref,
     mlp_gain_ref,
     out_ref,
+    latent_v,
+    rope_key_v,
+    key_up_v,
+    value_up_v,
+    inner_v,
+    outer_v,
+    qn_v,
+    qr_v,
+    stream_v,
+    q_ref,
     kv,
     weights,
     proj,
@@ -221,10 +239,26 @@
 ):
     t = Torus()
     me, x = t.me, t.x
+    depth = weights.shape[1] // 3
     loads = [
-        pltpu.make_async_copy(slab_hbm, kv.at[me], load_sems.at[0]),
-        pltpu.make_async_copy(proj_hbm, proj.at[x], load_sems.at[1]),
-        pltpu.make_async_copy(weights_hbm, weights.at[me], load_sems.at[2]),
+        pltpu.make_async_copy(src, dst, load_sems.at[n])
+        for n, (src, dst) in enumerate(
+            (
+                (latent_hbm, latent_v),
+                (key_up_hbm, key_up_v),
+                (value_up_hbm, value_up_v),
+                (rope_key_hbm, rope_key_v),
+                (inner_hbm, inner_v),
+                (outer_hbm.at[me], outer_v),
+                (proj_hbm, proj.at[x]),
+                (qn_hbm, qn_v),
+                (qr_hbm, qr_v),
+                (down_hbm, weights.at[me, pl.ds(2 * depth, depth)]),
+                (gate_hbm, weights.at[me, pl.ds(0, depth)]),
+                (up_hbm, weights.at[me, pl.ds(depth, depth)]),
+                (stream_hbm, stream_v),
+            )
+        )
     ]
     for load in loads:
         load.start()
@@ -234,7 +268,6 @@
     barrier = pltpu.get_barrier_semaphore()
     for peer in peers:
         pl.semaphore_signal(barrier, inc=1, device_id=peer, device_id_type=MESH)
-    pl.semaphore_wait(barrier, len(peers))
 
     pieces = Gather(t, kv, kv_send, kv_recv, kv_twin)
     halves = Gather(t, weights, w_send, w_recv, w_twin)
@@ -266,68 +299,100 @@
         ref = proj.at[slot, pl.ds(pl.multiple_of(first, share), share)]
         return remote(ref, ref, proj_send.at[0], proj_recv.at[recv], t.twin())
 
-    loads[0].wait()
+    for load in loads[:6]:
+        load.wait()
+    wide = latent_v[...].astype(F32)
+    factor = lax.rsqrt(jnp.mean(wide * wide, axis=-1, keepdims=True) + norm_floor)
+    normed = (wide * factor * latent_gain_ref[...]).astype(BF16)
+    slab = kv.at[me]
+    keys = jnp.dot(normed, key_up_v[...], preferred_element_type=F32).astype(BF16)
+    values = jnp.dot(normed, value_up_v[...], preferred_element_type=F32)
+    for h in range(2):
+        slab[h * rows : (h + 1) * rows, :] = keys[:, 128 * h : 128 * (h + 1)]
+        turned = values[:, 128 * h : 128 * (h + 1)].T.astype(BF16)
+        for i in range(rows // 128):
+            at = 2 * rows + h * rows + 128 * i
+            slab[at : at + 128, :] = turned[:, 128 * i : 128 * (i + 1)]
+    outer_cos, outer_sin = outer_v[0, :, 0:1], outer_v[1, :, 0:1]
+    inner_cos, inner_sin = inner_v[0], inner_v[1]
+    cosine = outer_cos * inner_cos - outer_sin * inner_sin
+    sine = outer_sin * inner_cos + outer_cos * inner_sin
+    mid = rows // 2
+    key_turned = turn(rope_key_v[...].astype(F32), cosine, sine).T
+    slab[4 * rows : 4 * rows + mid, :] = jnp.concatenate([key_turned[:mid], key_turned[mid:]], axis=1).astype(BF16)
+
+    pl.semaphore_wait(barrier, len(peers))
     pieces.send(0)
-    loads[1].wait()
+    loads[6].wait()
     for copy in proj_first:
         copy.start()
+
+    for load in loads[7:]:
+        load.wait()
+    zeros = jnp.zeros((64, rows), BF16)
+    for h in range(2):
+        nope = qn_v[:, h, :].astype(F32).T.astype(BF16)
+        rotary = turn(qr_v[64 * h : 64 * (h + 1), :].astype(F32), cosine, sine).astype(BF16)
+        for odd in range(2):
+            q_ref[2 * h + odd, 0:128, :] = nope
+            q_ref[2 * h + odd, 128:192, :] = zeros if odd else rotary
+            q_ref[2 * h + odd, 192:256, :] = rotary if odd else zeros
 
     m_ref[...] = jnp.full_like(m_ref, big_negative)
     l_ref[...] = jnp.zeros_like(l_ref)
     acc_ref[...] = jnp.zeros_like(acc_ref)
-    attend_chunk(kv.at[me], q_ref, m_ref, l_ref, acc_ref, rows, const, True)
-    loads[2].wait()
+    attend([kv.at[me]], q_ref, m_ref, l_ref, acc_ref, rows, const, diag=True)
+
+    last = len(ITEMS)
 
     def step(i, carry):
-        item = i // 2
-        odd = lax.rem(i, 2)
-        for k in range(1, len(ITEMS)):
-
-            @pl.when(i == 2 * (k - 1))
+        for group in range(0, last, 4):
+
+            @pl.when(i // 4 == group // 4)
             def _():
-                pieces.arrived(k)
-                pieces.send(k)
-
-        @pl.when(i == PROJ_SECOND)
+                for k in range(max(group, 1), group + 4):
+
+                    @pl.when(i == k)
+                    def _():
+                        pieces.arrived(k)
+                        pieces.send(k)
+                        if k == PROJ_SECOND:
+                            proj_copy(-1, None, 0, 0, minus).wait_recv()
+                            proj_copy(1, None, 0, 1, minus).wait_recv()
+                            for copy in proj_second:
+                                copy.start()
+                        if k == PROJ_THIRD:
+                            proj_copy(2, 0, 0, 2, minus).wait_recv()
+                            proj_copy(2, 1, 0, 3, minus).wait_recv()
+                            for copy in proj_third:
+                                copy.start()
+                        if k == WEIGHTS_FIRST:
+                            halves.send(0)
+
+        da, db, ea, eb = (jnp.int32(0) for _ in range(4))
+        for k, (ka, kb) in enumerate(ITEMS):
+            da = jnp.where(i == k, ka, da)
+            db = jnp.where(i == k, kb, db)
+            ea = jnp.where(i == k + 1, ka, ea)
+            eb = jnp.where(i == k + 1, kb, eb)
+        own_slot = t.index(da, db)
+        twin_slot = t.twin_index(ea, eb)
+        pieces.twin_arrived(i - 1, twin_slot)
+        own_here = jnp.logical_and(own_slot < me, i < last)
+        twin_here = twin_slot < me
+
+        @pl.when(jnp.logical_and(own_here, twin_here))
         def _():
-            proj_copy(-1, None, 0, 0, minus).wait_recv()
-            proj_copy(1, None, 0, 1, minus).wait_recv()
-            for copy in proj_second:
-                copy.start()
-
-        @pl.when(i == PROJ_THIRD)
+            attend([kv.at[own_slot], kv.at[twin_slot]], q_ref, m_ref, l_ref, acc_ref, rows, const)
+
+        @pl.when(own_here != twin_here)
         def _():
-            proj_copy(2, 0, 0, 2, minus).wait_recv()
-            proj_copy(2, 1, 0, 3, minus).wait_recv()
-            for copy in proj_third:
-                copy.start()
-
-        @pl.when(i == WEIGHTS_FIRST)
-        def _():
-            halves.send(0)
-
-        da, db = jnp.int32(0), jnp.int32(0)
-        number = item + 1 - odd
-        for k, (ka, kb) in enumerate(ITEMS):
-            da = jnp.where(number == k, ka, da)
-            db = jnp.where(number == k, kb, db)
-        off_a = jnp.where(odd == 1, db, da)
-        off_b = jnp.where(odd == 1, da, db)
-        at_a = lax.rem(t.a + off_a + 4, 4)
-        at_b = lax.rem(t.b + off_b + 4, 4)
-        slot = at_a * t.step_a + at_b * t.step_b + jnp.where(odd == 1, 1 - t.c, t.c)
-
-        @pl.when(odd == 1)
-        def _():
-            pieces.twin_arrived(item, slot)
-
-        @pl.when(jnp.logical_and(slot < me, i != STEPS - 2))
-        def _():
-            attend_chunk(kv.at[slot], q_ref, m_ref, l_ref, acc_ref, rows, const, False)
+            slot = jnp.where(own_here, own_slot, twin_slot)
+            attend([kv.at[slot]], q_ref, m_ref, l_ref, acc_ref, rows, const)
 
         return carry
 
-    lax.fori_loop(0, STEPS, step, 0)
+    lax.fori_loop(1, last + 1, step, 0)
 
     for h in range(2):
         attended[:, 128 * h : 128 * (h + 1)] = (acc_ref[h] / l_ref[h]).T.astype(BF16)
@@ -369,7 +434,7 @@
 
     lax.fori_loop(0, width // 256, project, 0)
     mixed[x] = layer_norm(
-        residual_weight * stream_ref[...].astype(F32) + sums[pl.ds(0, own), :], mix_gain_ref[...]
+        residual_weight * stream_v[...].astype(F32) + sums[pl.ds(0, own), :], mix_gain_ref[...]
     ).astype(BF16)
 
     half = own // 2
@@ -396,7 +461,6 @@
         halves.twin_arrived(k, t.twin_index(*item))
 
     count = weights.shape[0]
-    depth = weights.shape[1] // 3
     units = weights.shape[2]
 
     def feed(first, second):
@@ -404,28 +468,19 @@
             [mixed[lax.rem(x + first + 4, 4)], mixed[lax.rem(x + second + 4, 4)]], axis=0
         )
 
-        def expand(n, carry):
-            cols = pl.ds(pl.multiple_of(n * 256, 256), 256)
-            gate = jnp.dot(
-                into, weights[:, 0:depth, cols].reshape(count * depth, 256), preferred_element_type=F32
-            )
-            up = jnp.dot(
-                into, weights[:, depth : 2 * depth, cols].reshape(count * depth, 256), preferred_element_type=F32
-            )
-            hidden[:, cols] = (gate / (1.0 + jnp.exp(-gate)) * up).astype(BF16)
-            return carry
-
-        lax.fori_loop(0, units // 256, expand, 0)
-        group = 256 // depth
-
-        def lower(n, carry):
-            rhs = weights[pl.ds(n * group, group), 2 * depth : 3 * depth, :].reshape(256, units)
-            sums[:, pl.ds(pl.multiple_of(n * 256, 256), 256)] = lax.dot_general(
-                hidden[...], rhs, (((1,), (1,)), ((), ())), preferred_element_type=F32
-            )
-            return carry
-
-        lax.fori_loop(0, count // group, lower, 0)
+        gate = jnp.dot(
+            into, weights[:, 0:depth, :].reshape(count * depth, units), preferred_element_type=F32
+        )
+        up = jnp.dot(
+            into, weights[:, depth : 2 * depth, :].reshape(count * depth, units), preferred_element_type=F32
+        )
+        hidden[...] = (gate / (1.0 + jnp.exp(-gate)) * up).astype(BF16)
+        sums[...] = lax.dot_general(
+            hidden[...],
+            weights[:, 2 * depth : 3 * depth, :].reshape(count * depth, units),
+            (((1,), (1,)), ((), ())),
+            preferred_element_type=F32,
+        )
 
     top, low = pl.ds(0, half), pl.ds(half, half)
 
@@ -469,9 +524,9 @@
         copy.wait_send()
 
 
-PROJ_SECOND = 11
-PROJ_THIRD = 19
-WEIGHTS_FIRST = 23
+PROJ_SECOND = 5
+PROJ_THIRD = 9
+WEIGHTS_FIRST = 12
 
 
 def per_device(
@@ -496,40 +551,31 @@
     tp = lax.axis_size("tp")
     own, width = stream.shape
     units = w_gate.shape[1]
-    first_row = lax.axis_index("sp") * rows
-    query_turned = rotate(queries_rope.astype(F32), first_row).astype(BF16)
-    key_turned = rotate(rope_key.astype(F32), first_row).astype(BF16)
-    normed = latent_norm(latent, latent_gain)
-    keys = jnp.dot(normed, key_up, preferred_element_type=F32).astype(BF16)
-    values_t = lax.dot_general(
-        value_up, normed, (((0,), (1,)), ((), ())), preferred_element_type=F32
-    ).astype(BF16)
-    half = rows // 2
-    slab = jnp.concatenate(
-        [keys[:, :128], keys[:, 128:]]
-        + [values_t[128 * h : 128 * (h + 1), 128 * i : 128 * (i + 1)] for h in range(2) for i in range(rows // 128)]
-        + [jnp.concatenate([key_turned[:half], key_turned[half:]], axis=1)],
-        axis=0,
-    )
-    weights = jnp.concatenate([w_gate, w_up, w_down.T], axis=0)
-    qn = jnp.transpose(queries_nope, (1, 2, 0))
-    qr = jnp.transpose(query_turned, (1, 2, 0))
-    zero = jnp.zeros_like(qr)
-    q_all = jnp.stack(
-        [jnp.concatenate([qn, qr, zero], axis=1), jnp.concatenate([qn, zero, qr], axis=1)], axis=1
-    ).reshape(2 * heads, 2 * head_dim, rows)
     const = (head_dim + rope_dim) ** (-0.5) * math.log2(math.e)
+    lanes = heads * rope_dim
+    inner, outer = turn_tables(rows, count, rope_dim)
+    slab = 4 * rows + rows // 2
     vmem = pl.BlockSpec(memory_space=pltpu.VMEM)
     hbm = pl.BlockSpec(memory_space=pl.ANY)
     dma = pltpu.SemaphoreType.DMA
     return pl.pallas_call(
         functools.partial(whole_kernel, rows, const),
         out_shape=jax.ShapeDtypeStruct((own, width), BF16),
-        in_specs=[hbm, hbm, hbm, vmem, vmem, vmem, vmem],
+        in_specs=[hbm] * 13 + [vmem] * 3,
         out_specs=vmem,
         scratch_shapes=[
-            pltpu.VMEM((count, *slab.shape), BF16),
-            pltpu.VMEM((count, *weights.shape), BF16),
+            pltpu.VMEM(latent.shape, BF16),
+            pltpu.VMEM((rope_dim, rows), BF16),
+            pltpu.VMEM(key_up.shape, BF16),
+            pltpu.VMEM(value_up.shape, BF16),
+            pltpu.VMEM(inner.shape, F32),
+            pltpu.VMEM(outer.shape[1:], F32),
+            pltpu.VMEM(queries_nope.shape, BF16),
+            pltpu.VMEM((lanes, rows), BF16),
+            pltpu.VMEM((own, width), BF16),
+            pltpu.VMEM((2 * heads, 2 * head_dim, rows), BF16),
+            pltpu.VMEM((count, slab, 128), BF16),
+            pltpu.VMEM((count, 3 * w_gate.shape[0], units), BF16),
             pltpu.VMEM((tp, *out_proj.shape), BF16),
             pltpu.VMEM((2, 1, rows), F32),
             pltpu.VMEM((2, 1, rows), F32),
@@ -546,7 +592,7 @@
             pltpu.VMEM((own // 2, width), BF16),
             pltpu.VMEM((own, width), BF16),
             pltpu.VMEM((own, width), BF16),
-            dma((3,)),
+            dma((13,)),
             dma((16, 5)),
             dma((16, 2)),
             dma((16,)),
@@ -562,7 +608,24 @@
             collective_id=0, has_side_effects=True, vmem_limit_bytes=60 * 1024 * 1024
         ),
         name="layer",
-    )(slab, weights, out_proj, q_all, stream, mix_gain.reshape(1, -1), mlp_gain.reshape(1, -1))
+    )(
+        latent,
+        rope_key.T,
+        key_up,
+        value_up,
+        inner,
+        queries_nope,
+        jnp.transpose(queries_rope, (1, 2, 0)).reshape(lanes, rows),
+        out_proj,
+        w_gate,
+        w_up,
+        w_down.T,
+        stream,
+        outer,
+        latent_gain.reshape(1, -1),
+        mix_gain.reshape(1, -1),
+        mlp_gain.reshape(1, -1),
+    )
 
 
 def solution(mesh):

time: 117 us -> 99.4 us (0.85)
  local copies, waits for them, and re-layouts: 7.76 us -> 1.77 us
  other arithmetic: 5.5 us -> 0 us
  Pallas kernels: 101 us -> 97.2 us
    pallas_call x1, Pallas kernels: 101 us -> 97.2 us  [per_device(): pl.pallas_call(functools.partial(whole_kernel, rows, const), out_shape=ja...]
    unnamed x32 -> x1, local copies, waits for them, and re-layouts: 5.43 us -> 1.77 us
    another operation x3 -> x0, other arithmetic: 2.44 us -> none  [the longest x2 2.41 us: per_device(): jnp.stack([jnp.concatenate([qn, qr, zero], axis=1), jnp.concatenate([qn,...]
    another operation x1 -> x0, local copies, waits for them, and re-layouts: 1.85 us -> none  [per_device(): jnp.stack([jnp.concatenate([qn, qr, zero], axis=1), jnp.concatenate([qn,...]
    reduce_sum x1 -> x0, other arithmetic: 1.22 us -> none  [latent_norm(): jnp.mean(wide * wide, axis=-1, keepdims=True) + norm_floor]
where the time goes in v3:
time: 99.4 us; the launch traced here: 98.9 us
  Pallas kernels  97.2 us (98%)
  local copies, waits for them, and re-layouts  1.77 us (2%)
    pallas_call x1, Pallas kernels, per_device(): pl.pallas_call(functools.partial(whole_kernel, rows, const), out_shape=ja...  97.2 us

profile of v3, /device:TPU:1, one launch (start us, length us, event | category | flops | bytes accessed | tf_op | source)
XLA Modules:
  0.0 98.9 jit_solution(4310274368060057775)
XLA Ops:
  0.0 97.2 %layer.1 = bf16[96,2048]{1,0:T(8,128)(2,1)} custom-call(bf16[384,512]{1,0:T(8,128)(2,1)} %latent_hbm.1, bf16[64,384]{1,0:T(8,128)(2,1)} %bitcast.10, bf16[512,256]{1,0:T(8,128)(2,1)} %key_up_hbm.1, bf16[512,256]{1,0:T(8,128)(2,1)} %value_up_hbm.1, f32[2,32,384]{2,1,0:T(8,128)} %constant.4.clone.inner_hbm, bf16[384,2,128]{2,1,0:T(2,128)(2,1)} %qn_hbm.1, ...), custom_call_target="tpu_custom_call" | custom-call | tf_op jit(solution)/shard_map/layer/pallas_call | solution.py:561
  97.2 1.8 %copy.18 = bf16[96,2048]{1,0:T(8,128)(2,1)} copy(bf16[96,2048]{1,0:T(8,128)(2,1)} %layer.1) | data formatting | bytes 786432

commit v4 on v3

--- a/solution.py
+++ b/solution.py
@@ -119,62 +119,61 @@
 
 
 class Gather:
-    def __init__(self, torus, buf, send_sems, recv_sems, twin_sems):
-        self.torus, self.buf = torus, buf
-        self.send_sems, self.recv_sems, self.twin_sems = send_sems, recv_sems, twin_sems
-        self.half = buf.shape[1] // 2
-
-    def part(self, slot, which):
-        if which is None:
-            return self.buf.at[slot]
-        return self.buf.at[slot, pl.ds(which * self.half, self.half)]
-
-    def copies(self, k):
+    def __init__(self, torus, buf, parts, send_sem, recv_sems, twin_sems, twin_of):
+        self.torus, self.buf, self.parts = torus, buf, parts
+        self.send_sem, self.recv_sems, self.twin_sems, self.twin_of = send_sem, recv_sems, twin_sems, twin_of
+
+    def ref(self, slot, part, which=None):
+        begin, size = self.parts[part]
+        if which is not None:
+            size //= 2
+            begin += which * size
+        return self.buf.at[slot, pl.ds(begin, size)]
+
+    def copies(self, k, part):
         t = self.torus
         da, db = ITEMS[k]
         slot = t.index(da, db)
         plan = []
         if db == 0:
             if da == 0:
-                plan += [(2, (1, 0), (-1, 0), None), (3, (-1, 0), (1, 0), None)]
-            plan += [(0, (0, 1), (da, -1), None), (1, (0, -1), (da, 1), None)]
+                plan += [((1, 0), (-1, 0), None), ((-1, 0), (1, 0), None)]
+            plan += [((0, 1), (da, -1), None), ((0, -1), (da, 1), None)]
             if da == -1:
-                plan += [(2, (1, 0), (2, 0), 0)]
+                plan += [((1, 0), (2, 0), 0)]
             if da == 1:
-                plan += [(2, (-1, 0), (2, 0), 1)]
+                plan += [((-1, 0), (2, 0), 1)]
         if db == -1:
-            plan += [(0, (0, 1), (da, 2), 0)]
+            plan += [((0, 1), (da, 2), 0)]
         if db == 1:
-            plan += [(1, (0, -1), (da, 2), 1)]
+            plan += [((0, -1), (da, 2), 1)]
         out = []
-        for sem, to, name, which in plan:
-            ref = self.part(slot, which)
-            recv = self.recv_sems.at[PLACE[name], which or 0]
-            out.append(remote(ref, ref, self.send_sems.at[k, sem], recv, t.at(*to)))
-        ref = self.part(slot, None)
-        out.append(remote(ref, ref, self.send_sems.at[k, 4], self.twin_sems.at[k], t.twin()))
+        for to, name, which in plan:
+            ref = self.ref(slot, part, which)
+            out.append(remote(ref, ref, self.send_sem, self.recv_sems.at[PLACE[name], part], t.at(*to)))
+        ref = self.ref(slot, part)
+        out.append(remote(ref, ref, self.send_sem, self.twin_sems.at[self.twin_of(k)], t.twin()))
         return out
 
-    def send(self, k):
-        for copy in self.copies(k):
+    def send(self, k, part):
+        for copy in self.copies(k, part):
             copy.start()
 
     def sent(self):
-        for k in range(len(ITEMS)):
-            for copy in self.copies(k):
-                copy.wait_send()
-
-    def arrived(self, k):
-        t = self.torus
-        da, db = ITEMS[k]
-        slot = t.index(da, db)
-        for which in (0, 1) if 2 in (da, db) and not (da == 2 and db in (-1, 1)) else (None,):
-            ref = self.part(slot, which)
-            remote(ref, ref, self.send_sems.at[k, 0], self.recv_sems.at[k, which or 0], t.twin()).wait_recv()
-
-    def twin_arrived(self, k, slot):
-        ref = self.part(slot, None)
-        remote(ref, ref, self.send_sems.at[0, 0], self.twin_sems.at[k], self.torus.twin()).wait_recv()
+        ref = self.buf.at[pl.ds(0, 31)]
+        remote(ref, ref, self.send_sem, self.recv_sems.at[0, 0], self.torus.twin()).wait_send()
+
+    def arrived(self, k, part):
+        ref = self.ref(self.torus.index(*ITEMS[k]), part)
+        remote(ref, ref, self.send_sem, self.recv_sems.at[k, part], self.torus.twin()).wait_recv()
+
+    def pass_on(self, k, part):
+        self.arrived(k, part)
+        self.send(k, part)
+
+    def twin_arrived(self, sem, first, count):
+        ref = self.buf.at[pl.ds(first, count)]
+        remote(ref, ref, self.send_sem, self.twin_sems.at[sem], self.torus.twin()).wait_recv()
 
 
 def whole_kernel(
@@ -205,7 +204,6 @@
     outer_v,
     qn_v,
     qr_v,
-    stream_v,
     q_ref,
     kv,
     weights,
@@ -213,11 +211,13 @@
     m_ref,
     l_ref,
     acc_ref,
-    attended,
-    row_heads,
+    heads_all,
+    stream_all,
     sums,
     mixed,
     hidden,
+    gate_sum,
+    up_sum,
     far_out,
     plus_out,
     minus_out,
@@ -234,6 +234,8 @@
     w_twin,
     proj_send,
     proj_recv,
+    ring_send,
+    ring_recv,
     x_send,
     x_recv,
 ):
@@ -256,7 +258,7 @@
                 (down_hbm, weights.at[me, pl.ds(2 * depth, depth)]),
                 (gate_hbm, weights.at[me, pl.ds(0, depth)]),
                 (up_hbm, weights.at[me, pl.ds(depth, depth)]),
-                (stream_hbm, stream_v),
+                (stream_hbm, stream_all.at[x]),
             )
         )
     ]
@@ -269,8 +271,45 @@
     for peer in peers:
         pl.semaphore_signal(barrier, inc=1, device_id=peer, device_id_type=MESH)
 
-    pieces = Gather(t, kv, kv_send, kv_recv, kv_twin)
-    halves = Gather(t, weights, w_send, w_recv, w_twin)
+    slab_rows = kv.shape[1]
+    pieces = Gather(t, kv, [(0, slab_rows // 2), (slab_rows // 2, slab_rows // 2)], kv_send.at[0], kv_recv, kv_twin, lambda k: k)
+    halves = Gather(t, weights, [(0, 3 * depth)], w_send.at[0], w_recv, w_twin, lambda k: k // EARLY)
+
+    class Ring:
+        def __init__(self, buf, send_sem, first_sem):
+            self.buf, self.send_sem, self.first_sem, self.half = buf, send_sem, first_sem, buf.shape[1] // 2
+
+        def copy(self, d, which, sem, to):
+            ref = self.buf.at[lax.rem(x + d + 4, 4), pl.ds(which * self.half, self.half)]
+            n = self.first_sem + sem
+            return remote(ref, ref, self.send_sem, ring_recv.at[n], to)
+
+        def first(self):
+            return [
+                self.copy(0, 0, 0, plus),
+                self.copy(0, 1, 1, minus),
+                self.copy(0, 1, 2, plus),
+                self.copy(0, 0, 3, minus),
+            ]
+
+        def second(self, which):
+            return self.copy(1, 1, 5, minus) if which else self.copy(-1, 0, 4, plus)
+
+        def forward(self):
+            for d, which in ((-1, 0), (1, 1)):
+                self.copy(d, which, which, plus).wait_recv()
+                self.second(which).start()
+
+        def near_arrived(self):
+            self.copy(-1, 1, 2, plus).wait_recv()
+            self.copy(1, 0, 3, plus).wait_recv()
+
+        def far_arrived(self):
+            self.copy(2, 0, 4, plus).wait_recv()
+            self.copy(2, 1, 5, plus).wait_recv()
+
+    stream_ring = Ring(stream_all, ring_send.at[0], 0)
+    heads_ring = Ring(heads_all, ring_send.at[1], 6)
 
     share = proj.shape[1] // 2
 
@@ -282,7 +321,7 @@
 
     def proj_copy(d, which, sem, recv, to):
         ref = proj_part(d, which)
-        return remote(ref, ref, proj_send.at[sem], proj_recv.at[recv], to)
+        return remote(ref, ref, proj_send.at[0], proj_recv.at[recv], to)
 
     proj_first = [proj_copy(0, None, 0, 0, plus), proj_copy(0, None, 1, 1, minus)]
     proj_second = [
@@ -322,13 +361,16 @@
     slab[4 * rows : 4 * rows + mid, :] = jnp.concatenate([key_turned[:mid], key_turned[mid:]], axis=1).astype(BF16)
 
     pl.semaphore_wait(barrier, len(peers))
-    pieces.send(0)
+    for part in range(2):
+        pieces.send(0, part)
     loads[6].wait()
     for copy in proj_first:
         copy.start()
 
     for load in loads[7:]:
         load.wait()
+    for copy in stream_ring.first():
+        copy.start()
     zeros = jnp.zeros((64, rows), BF16)
     for h in range(2):
         nope = qn_v[:, h, :].astype(F32).T.astype(BF16)
@@ -354,8 +396,11 @@
 
                     @pl.when(i == k)
                     def _():
-                        pieces.arrived(k)
-                        pieces.send(k)
+                        for begin, end in GROUPS:
+                            if k == begin:
+                                for other in range(begin, end):
+                                    pieces.pass_on(other, 0)
+                        pieces.pass_on(k, 1)
                         if k == PROJ_SECOND:
                             proj_copy(-1, None, 0, 0, minus).wait_recv()
                             proj_copy(1, None, 0, 1, minus).wait_recv()
@@ -366,8 +411,9 @@
                             proj_copy(2, 1, 0, 3, minus).wait_recv()
                             for copy in proj_third:
                                 copy.start()
+                            stream_ring.forward()
                         if k == WEIGHTS_FIRST:
-                            halves.send(0)
+                            halves.send(0, 0)
 
         da, db, ea, eb = (jnp.int32(0) for _ in range(4))
         for k, (ka, kb) in enumerate(ITEMS):
@@ -377,7 +423,7 @@
             eb = jnp.where(i == k + 1, kb, eb)
         own_slot = t.index(da, db)
         twin_slot = t.twin_index(ea, eb)
-        pieces.twin_arrived(i - 1, twin_slot)
+        pieces.twin_arrived(i - 1, twin_slot, 1)
         own_here = jnp.logical_and(own_slot < me, i < last)
         twin_here = twin_slot < me
 
@@ -394,102 +440,80 @@
 
     lax.fori_loop(1, last + 1, step, 0)
 
+    own = rows // 4
     for h in range(2):
-        attended[:, 128 * h : 128 * (h + 1)] = (acc_ref[h] / l_ref[h]).T.astype(BF16)
-    own = rows // 4
-
-    def own_rows(d):
-        first = lax.rem(x + d + 4, 4) * own
-        return attended.at[pl.ds(pl.multiple_of(first, own), own)]
-
-    heads_out = [
-        remote(own_rows(2), row_heads.at[x], x_send.at[0], x_recv.at[0], across),
-        remote(own_rows(1), row_heads.at[x], x_send.at[1], x_recv.at[1], plus),
-        remote(own_rows(-1), row_heads.at[x], x_send.at[2], x_recv.at[2], minus),
-    ]
-    for copy in heads_out:
+        heads_all[x, :, 128 * h : 128 * (h + 1)] = (acc_ref[h] / l_ref[h]).T.astype(BF16)
+    for copy in heads_ring.first():
         copy.start()
-    row_heads[x] = attended[pl.ds(pl.multiple_of(x * own, own), own), :]
-
-    def weights_step(first, last):
-        for k in range(first, last):
-            halves.arrived(k)
-            halves.send(k)
-
-    weights_step(1, 3)
+    for k in range(1, 5):
+        halves.pass_on(k, 0)
+    stream_ring.near_arrived()
+    stream_ring.far_arrived()
     for d, sem in ((1, 4), (-1, 5), (2, 6)):
         twin_proj(d, sem).wait_recv()
-    for d, sem in ((2, 0), (-1, 1), (1, 2)):
-        ref = row_heads.at[lax.rem(x + d + 4, 4)]
-        remote(ref, ref, x_send.at[0], x_recv.at[sem], plus).wait_recv()
-
-    lhs = jnp.concatenate([row_heads[p] for p in range(4)], axis=1)
-    width = sums.shape[1]
-
-    def project(n, carry):
-        cols = pl.ds(pl.multiple_of(n * 256, 256), 256)
-        rhs = proj[:, :, cols].reshape(4 * proj.shape[1], 256)
-        sums[pl.ds(0, own), cols] = jnp.dot(lhs, rhs, preferred_element_type=F32)
+    heads_ring.forward()
+    heads_ring.near_arrived()
+
+    def slots(ref, offsets, axis):
+        return jnp.concatenate([ref[lax.rem(x + d + 4, 4)] for d in offsets], axis=axis)
+
+    halves.pass_on(5, 0)
+    near = (0, 1, -1)
+    sums[...] = jnp.dot(slots(heads_all, near, 1), slots(proj, near, 0), preferred_element_type=F32)
+    for k in range(6, 10):
+        halves.pass_on(k, 0)
+    heads_ring.far_arrived()
+    sums[...] += jnp.dot(slots(heads_all, (2,), 1), slots(proj, (2,), 0), preferred_element_type=F32)
+
+    def norm_rows(n, carry):
+        total = sums[pl.ds(pl.multiple_of(n * own, own), own), :]
+        mixed[n] = layer_norm(residual_weight * stream_all[n].astype(F32) + total, mix_gain_ref[...]).astype(BF16)
         return carry
 
-    lax.fori_loop(0, width // 256, project, 0)
-    mixed[x] = layer_norm(
-        residual_weight * stream_v[...].astype(F32) + sums[pl.ds(0, own), :], mix_gain_ref[...]
-    ).astype(BF16)
-
-    half = own // 2
-
-    def mixed_copy(d, which, sem, recv, to):
-        slot = lax.rem(x + d + 4, 4)
-        ref = mixed.at[slot] if which is None else mixed.at[slot, pl.ds(which * half, half)]
-        return remote(ref, ref, x_send.at[sem], x_recv.at[recv], to)
-
-    mixed_first = [mixed_copy(0, None, 3, 3, plus), mixed_copy(0, None, 4, 4, minus)]
-    mixed_second = [mixed_copy(-1, 0, 5, 5, plus), mixed_copy(1, 1, 6, 6, minus)]
-    for copy in mixed_first:
-        copy.start()
-    weights_step(3, 10)
-    mixed_copy(-1, None, 3, 3, plus).wait_recv()
-    mixed_copy(1, None, 3, 4, plus).wait_recv()
-    for copy in mixed_second:
-        copy.start()
-    weights_step(10, 13)
-    mixed_copy(2, 0, 3, 5, plus).wait_recv()
-    mixed_copy(2, 1, 3, 6, plus).wait_recv()
-    weights_step(13, 16)
-    for k, item in enumerate(ITEMS):
-        halves.twin_arrived(k, t.twin_index(*item))
-
-    count = weights.shape[0]
-    units = weights.shape[2]
-
-    def feed(first, second):
+    lax.fori_loop(0, 4, norm_rows, 0)
+    count, units = weights.shape[0], weights.shape[2]
+    halves.pass_on(10, 0)
+    halves.twin_arrived(0, 0, EARLY)
+
+    def expand(items):
+        chips = [t.index(*item) // 2 for item in items]
         into = jnp.concatenate(
-            [mixed[lax.rem(x + first + 4, 4)], mixed[lax.rem(x + second + 4, 4)]], axis=0
+            [mixed[:, :, pl.ds(pl.multiple_of(chip * 2 * depth, 2 * depth), 2 * depth)].reshape(rows, 2 * depth) for chip in chips],
+            axis=1,
         )
 
-        gate = jnp.dot(
-            into, weights[:, 0:depth, :].reshape(count * depth, units), preferred_element_type=F32
-        )
-        up = jnp.dot(
-            into, weights[:, depth : 2 * depth, :].reshape(count * depth, units), preferred_element_type=F32
-        )
-        hidden[...] = (gate / (1.0 + jnp.exp(-gate)) * up).astype(BF16)
-        sums[...] = lax.dot_general(
-            hidden[...],
+        def rhs(begin):
+            blocks = [weights[pl.ds(chip * 2, 2), begin : begin + depth, :].reshape(2 * depth, units) for chip in chips]
+            return jnp.concatenate(blocks, axis=0)
+
+        return [jnp.dot(into, rhs(begin), preferred_element_type=F32) for begin in (0, depth)]
+
+    gate_sum[...], up_sum[...] = expand(ITEMS[:EARLY])
+    for k in range(EARLY, 16):
+        halves.pass_on(k, 0)
+    halves.twin_arrived(1, 0, 16 - EARLY)
+    gate, up = expand(ITEMS[EARLY:])
+    gate = gate_sum[...] + gate
+    hidden[...] = (gate / (1.0 + jnp.exp(-gate)) * (up_sum[...] + up)).astype(BF16)
+
+    def lower(first, second):
+        rows_of = [hidden[pl.ds(pl.multiple_of(lax.rem(x + d + 4, 4) * own, own), own), :] for d in (first, second)]
+        sums[0 : 2 * own, :] = lax.dot_general(
+            jnp.concatenate(rows_of, axis=0),
             weights[:, 2 * depth : 3 * depth, :].reshape(count * depth, units),
             (((1,), (1,)), ((), ())),
             preferred_element_type=F32,
         )
 
+    half = own // 2
     top, low = pl.ds(0, half), pl.ds(half, half)
 
     def result_copy(src, src_rows, dst, dst_rows, sem, to):
         s = src.at[src_rows]
         d = dst if dst_rows is None else dst.at[dst_rows]
-        return remote(s, d, x_send.at[sem], x_recv.at[sem], to)
-
-    feed(2, 1)
+        return remote(s, d, x_send.at[0], x_recv.at[sem - 7], to)
+
+    lower(2, 1)
     far_out[...] = sums[0:own, :].astype(BF16)
     plus_out[...] = sums[own : 2 * own, :].astype(BF16)
     back = [
@@ -502,7 +526,7 @@
     ]
     for copy in back[:3]:
         copy.start()
-    feed(-1, 0)
+    lower(-1, 0)
     minus_out[...] = sums[0:own, :].astype(BF16)
     back[3].start()
     back[0].wait_recv()
@@ -520,10 +544,17 @@
 
     pieces.sent()
     halves.sent()
-    for copy in proj_first + proj_second + proj_third + heads_out + mixed_first + mixed_second + back:
-        copy.wait_send()
-
-
+    for ref, sem in (
+        (proj.at[pl.ds(0, 3)], proj_send.at[0]),
+        (stream_all.at[pl.ds(0, 3)], ring_send.at[0]),
+        (heads_all.at[pl.ds(0, 3)], ring_send.at[1]),
+        (mixed.at[pl.ds(0, 3)], x_send.at[0]),
+    ):
+        remote(ref, ref, sem, x_recv.at[0], t.twin()).wait_send()
+
+
+GROUPS = ((1, 5), (5, 11), (11, 15), (15, 16))
+EARLY = 11
 PROJ_SECOND = 5
 PROJ_THIRD = 9
 WEIGHTS_FIRST = 12
@@ -572,7 +603,6 @@
             pltpu.VMEM(outer.shape[1:], F32),
             pltpu.VMEM(queries_nope.shape, BF16),
             pltpu.VMEM((lanes, rows), BF16),
-            pltpu.VMEM((own, width), BF16),
             pltpu.VMEM((2 * heads, 2 * head_dim, rows), BF16),
             pltpu.VMEM((count, slab, 128), BF16),
             pltpu.VMEM((count, 3 * w_gate.shape[0], units), BF16),
@@ -580,11 +610,13 @@
             pltpu.VMEM((2, 1, rows), F32),
             pltpu.VMEM((2, 1, rows), F32),
             pltpu.VMEM((2, 128, rows), F32),
-            pltpu.VMEM((rows, heads * head_dim), BF16),
-            pltpu.VMEM((tp, own, heads * head_dim), BF16),
-            pltpu.VMEM((2 * own, width), F32),
+            pltpu.VMEM((tp, rows, heads * head_dim), BF16),
             pltpu.VMEM((tp, own, width), BF16),
-            pltpu.VMEM((2 * own, units), BF16),
+            pltpu.VMEM((rows, width), F32),
+            pltpu.VMEM((tp, own, width), BF16),
+            pltpu.VMEM((rows, units), BF16),
+            pltpu.VMEM((rows, units), F32),
+            pltpu.VMEM((rows, units), F32),
             pltpu.VMEM((own, width), BF16),
             pltpu.VMEM((own, width), BF16),
             pltpu.VMEM((own, width), BF16),
@@ -593,16 +625,18 @@
             pltpu.VMEM((own, width), BF16),
             pltpu.VMEM((own, width), BF16),
             dma((13,)),
-            dma((16, 5)),
+            dma((1,)),
             dma((16, 2)),
             dma((16,)),
-            dma((16, 5)),
-            dma((16, 2)),
-            dma((16,)),
+            dma((1,)),
+            dma((16, 1)),
+            dma((2,)),
+            dma((1,)),
             dma((7,)),
-            dma((7,)),
-            dma((13,)),
-            dma((13,)),
+            dma((2,)),
+            dma((12,)),
+            dma((1,)),
+            dma((6,)),
         ],
         compiler_params=pltpu.CompilerParams(
             collective_id=0, has_side_effects=True, vmem_limit_bytes=60 * 1024 * 1024

time: 99.4 us -> 94.1 us (0.947)
  Pallas kernels: 97.2 us -> 92.1 us
    pallas_call x1, Pallas kernels: 97.2 us -> 92.1 us  [per_device(): pl.pallas_call(functools.partial(whole_kernel, rows, const), out_shape=ja...]
where the time goes in v4:
time: 94.1 us; the launch traced here: 93.9 us
  Pallas kernels  92.1 us (98%)
  local copies, waits for them, and re-layouts  1.77 us (2%)
    pallas_call x1, Pallas kernels, per_device(): pl.pallas_call(functools.partial(whole_kernel, rows, const), out_shape=ja...  92.1 us

profile of v4, /device:TPU:1, one launch (start us, length us, event | category | flops | bytes accessed | tf_op | source)
XLA Modules:
  0.0 93.9 jit_solution(2977122457254960511)
XLA Ops:
  0.0 92.1 %layer.1 = bf16[96,2048]{1,0:T(8,128)(2,1)} custom-call(bf16[384,512]{1,0:T(8,128)(2,1)} %latent_hbm.1, bf16[64,384]{1,0:T(8,128)(2,1)} %bitcast.10, bf16[512,256]{1,0:T(8,128)(2,1)} %key_up_hbm.1, bf16[512,256]{1,0:T(8,128)(2,1)} %value_up_hbm.1, f32[2,32,384]{2,1,0:T(8,128)} %constant.4.clone.inner_hbm, bf16[384,2,128]{2,1,0:T(2,128)(2,1)} %qn_hbm.1, ...), custom_call_target="tpu_custom_call" | custom-call | tf_op jit(solution)/shard_map/layer/pallas_call | solution.py:592
  92.1 1.8 %copy.18 = bf16[96,2048]{1,0:T(8,128)(2,1)} copy(bf16[96,2048]{1,0:T(8,128)(2,1)} %layer.1) | data formatting | bytes 786432

commit v5 on v4

--- a/solution.py
+++ b/solution.py
@@ -152,7 +152,7 @@
             ref = self.ref(slot, part, which)
             out.append(remote(ref, ref, self.send_sem, self.recv_sems.at[PLACE[name], part], t.at(*to)))
         ref = self.ref(slot, part)
-        out.append(remote(ref, ref, self.send_sem, self.twin_sems.at[self.twin_of(k)], t.twin()))
+        out.append(remote(ref, ref, self.send_sem, self.twin_sems.at[self.twin_of(k, part)], t.twin()))
         return out
 
     def send(self, k, part):
@@ -171,8 +171,10 @@
         self.arrived(k, part)
         self.send(k, part)
 
-    def twin_arrived(self, sem, first, count):
+    def twin_arrived(self, sem, first, count, part=None):
         ref = self.buf.at[pl.ds(first, count)]
+        if part is not None:
+            ref = self.buf.at[pl.ds(first, count), pl.ds(*self.parts[part])]
         remote(ref, ref, self.send_sem, self.twin_sems.at[sem], self.torus.twin()).wait_recv()
 
 
@@ -272,8 +274,8 @@
         pl.semaphore_signal(barrier, inc=1, device_id=peer, device_id_type=MESH)
 
     slab_rows = kv.shape[1]
-    pieces = Gather(t, kv, [(0, slab_rows // 2), (slab_rows // 2, slab_rows // 2)], kv_send.at[0], kv_recv, kv_twin, lambda k: k)
-    halves = Gather(t, weights, [(0, 3 * depth)], w_send.at[0], w_recv, w_twin, lambda k: k // EARLY)
+    pieces = Gather(t, kv, [(0, slab_rows // 2), (slab_rows // 2, slab_rows // 2)], kv_send.at[0], kv_recv, kv_twin, lambda k, part: k)
+    halves = Gather(t, weights, [(0, 2 * depth), (2 * depth, depth)], w_send.at[0], w_recv, w_twin, lambda k, part: 2 * part + k // EARLY)
 
     class Ring:
         def __init__(self, buf, send_sem, first_sem):
@@ -413,7 +415,8 @@
                                 copy.start()
                             stream_ring.forward()
                         if k == WEIGHTS_FIRST:
-                            halves.send(0, 0)
+                            for part in range(2):
+                                halves.send(0, part)
 
         da, db, ea, eb = (jnp.int32(0) for _ in range(4))
         for k, (ka, kb) in enumerate(ITEMS):
@@ -445,23 +448,26 @@
         heads_all[x, :, 128 * h : 128 * (h + 1)] = (acc_ref[h] / l_ref[h]).T.astype(BF16)
     for copy in heads_ring.first():
         copy.start()
-    for k in range(1, 5):
-        halves.pass_on(k, 0)
+
+    def pass_weights(first, last, part):
+        for k in range(first, last):
+            halves.pass_on(k, part)
+
+    pass_weights(1, 5, 0)
     stream_ring.near_arrived()
     stream_ring.far_arrived()
     for d, sem in ((1, 4), (-1, 5), (2, 6)):
         twin_proj(d, sem).wait_recv()
     heads_ring.forward()
+    pass_weights(5, 8, 0)
     heads_ring.near_arrived()
 
     def slots(ref, offsets, axis):
         return jnp.concatenate([ref[lax.rem(x + d + 4, 4)] for d in offsets], axis=axis)
 
-    halves.pass_on(5, 0)
     near = (0, 1, -1)
     sums[...] = jnp.dot(slots(heads_all, near, 1), slots(proj, near, 0), preferred_element_type=F32)
-    for k in range(6, 10):
-        halves.pass_on(k, 0)
+    pass_weights(8, 10, 0)
     heads_ring.far_arrived()
     sums[...] += jnp.dot(slots(heads_all, (2,), 1), slots(proj, (2,), 0), preferred_element_type=F32)
 
@@ -472,75 +478,111 @@
 
     lax.fori_loop(0, 4, norm_rows, 0)
     count, units = weights.shape[0], weights.shape[2]
-    halves.pass_on(10, 0)
-    halves.twin_arrived(0, 0, EARLY)
-
-    def expand(items):
-        chips = [t.index(*item) // 2 for item in items]
-        into = jnp.concatenate(
-            [mixed[:, :, pl.ds(pl.multiple_of(chip * 2 * depth, 2 * depth), 2 * depth)].reshape(rows, 2 * depth) for chip in chips],
-            axis=1,
-        )
-
-        def rhs(begin):
-            blocks = [weights[pl.ds(chip * 2, 2), begin : begin + depth, :].reshape(2 * depth, units) for chip in chips]
-            return jnp.concatenate(blocks, axis=0)
-
-        return [jnp.dot(into, rhs(begin), preferred_element_type=F32) for begin in (0, depth)]
-
-    gate_sum[...], up_sum[...] = expand(ITEMS[:EARLY])
-    for k in range(EARLY, 16):
-        halves.pass_on(k, 0)
-    halves.twin_arrived(1, 0, 16 - EARLY)
-    gate, up = expand(ITEMS[EARLY:])
-    gate = gate_sum[...] + gate
-    hidden[...] = (gate / (1.0 + jnp.exp(-gate)) * (up_sum[...] + up)).astype(BF16)
-
-    def lower(first, second):
-        rows_of = [hidden[pl.ds(pl.multiple_of(lax.rem(x + d + 4, 4) * own, own), own), :] for d in (first, second)]
-        sums[0 : 2 * own, :] = lax.dot_general(
-            jnp.concatenate(rows_of, axis=0),
-            weights[:, 2 * depth : 3 * depth, :].reshape(count * depth, units),
-            (((1,), (1,)), ((), ())),
-            preferred_element_type=F32,
-        )
+    pass_weights(10, 11, 0)
+    pass_weights(1, 5, 1)
+    pass_weights(11, 13, 0)
+    halves.twin_arrived(0, 0, EARLY, 0)
+
+    def weight_rows(chips, begin):
+        blocks = [weights[pl.ds(chip * 2, 2), begin : begin + depth, :].reshape(2 * depth, units) for chip in chips]
+        return jnp.concatenate(blocks, axis=0)
+
+    def expand(chips, into):
+        return [jnp.dot(into, weight_rows(chips, begin), preferred_element_type=F32) for begin in (0, depth)]
+
+    def columns(ref, chips):
+        n = ref.shape[0] if len(ref.shape) == 2 else ref.shape[0] * ref.shape[1]
+        cols = [ref.at[..., pl.ds(pl.multiple_of(chip * 2 * depth, 2 * depth), 2 * depth)] for chip in chips]
+        return jnp.concatenate([c[...].reshape(n, 2 * depth) for c in cols], axis=1)
+
+    chips = [t.index(*item) // 2 for item in ITEMS]
+    gate_sum[...], up_sum[...] = expand(chips[:EARLY], columns(mixed, chips[:EARLY]))
+    pass_weights(13, 15, 0)
+    pass_weights(5, 10, 1)
+    pass_weights(15, 16, 0)
+    halves.twin_arrived(1, 0, 16 - EARLY, 0)
+
+    def rows_at(d):
+        return pl.ds(pl.multiple_of(lax.rem(x + d + 4, 4) * own, own), own)
+
+    def activate(first, second):
+        into = [columns(mixed.at[lax.rem(x + d + 4, 4)], chips[EARLY:]) for d in (first, second)]
+        gate, up = expand(chips[EARLY:], jnp.concatenate(into, axis=0))
+        for n, d in enumerate((first, second)):
+            g = gate_sum[rows_at(d), :] + gate[n * own : (n + 1) * own]
+            u = up_sum[rows_at(d), :] + up[n * own : (n + 1) * own]
+            hidden[rows_at(d), :] = (g / (1.0 + jnp.exp(-g)) * u).astype(BF16)
+
+    activate(2, 1)
+    activate(-1, 0)
+    pass_weights(10, 13, 1)
+    halves.twin_arrived(2, 0, EARLY, 1)
 
     half = own // 2
     top, low = pl.ds(0, half), pl.ds(half, half)
-
-    def result_copy(src, src_rows, dst, dst_rows, sem, to):
-        s = src.at[src_rows]
-        d = dst if dst_rows is None else dst.at[dst_rows]
-        return remote(s, d, x_send.at[0], x_recv.at[sem - 7], to)
-
-    lower(2, 1)
-    far_out[...] = sums[0:own, :].astype(BF16)
-    plus_out[...] = sums[own : 2 * own, :].astype(BF16)
-    back = [
-        result_copy(far_out, top, far_minus, None, 7, plus),
-        result_copy(far_out, low, far_plus, None, 8, minus),
-        result_copy(plus_out, low, from_minus, low, 9, plus),
-        result_copy(minus_out, top, from_plus, top, 10, minus),
-        result_copy(plus_out, top, from_minus, top, 11, plus),
-        result_copy(minus_out, low, from_plus, low, 12, minus),
-    ]
-    for copy in back[:3]:
-        copy.start()
-    lower(-1, 0)
-    minus_out[...] = sums[0:own, :].astype(BF16)
-    back[3].start()
-    back[0].wait_recv()
-    plus_out[top, :] = (plus_out[top, :].astype(F32) + far_minus[...].astype(F32)).astype(BF16)
-    back[4].start()
-    back[1].wait_recv()
-    minus_out[low, :] = (minus_out[low, :].astype(F32) + far_plus[...].astype(F32)).astype(BF16)
-    back[5].start()
-    for copy in back[2:]:
-        copy.wait_recv()
-    lowered = sums[own : 2 * own, :] + from_plus[...].astype(F32) + from_minus[...].astype(F32)
-    out_ref[...] = layer_norm(
-        residual_weight * mixed[x].astype(F32) + 0.5 * lowered, mlp_gain_ref[...]
+    split = EARLY * 2 * depth
+    column_sets = [(chips[:EARLY], pl.ds(0, split)), (chips[EARLY:], pl.ds(split, sums.shape[1] - split))]
+
+    def lower(first, second, late):
+        lhs = jnp.concatenate([hidden[rows_at(first), :], hidden[rows_at(second), :]], axis=0)
+        rhs = weight_rows(column_sets[late][0], 2 * depth)
+        out = lax.dot_general(lhs, rhs, (((1,), (1,)), ((), ())), preferred_element_type=F32)
+        return out[:own], out[own:]
+
+    def back(n, late):
+        cols = column_sets[late][1]
+        src, src_rows, dst, dst_rows, recv, to = (
+            (far_out, top, far_minus, pl.ds(0, half), 2 * late, plus),
+            (far_out, low, far_plus, pl.ds(0, half), 2 * late + 1, minus),
+            (plus_out, low, from_minus, low, 4, plus),
+            (minus_out, top, from_plus, top, 5, minus),
+            (plus_out, top, from_minus, top, 4, plus),
+            (minus_out, low, from_plus, low, 5, minus),
+        )[n]
+        return remote(src.at[src_rows, cols], dst.at[dst_rows, cols], x_send.at[0], x_recv.at[recv], to)
+
+    def lower_far(late):
+        cols = column_sets[late][1]
+        far, near = lower(2, 1, late)
+        far_out[:, cols] = far.astype(BF16)
+        plus_out[:, cols] = near.astype(BF16)
+        back(0, late).start()
+        back(1, late).start()
+
+    def lower_near(late):
+        cols = column_sets[late][1]
+        near, here = lower(-1, 0, late)
+        minus_out[:, cols] = near.astype(BF16)
+        sums[0:own, cols] = here
+        back(2, late).start()
+        back(3, late).start()
+
+    def add_far(late):
+        cols = column_sets[late][1]
+        back(0, late).wait_recv()
+        plus_out[top, cols] = (plus_out[top, cols].astype(F32) + far_minus[:, cols].astype(F32)).astype(BF16)
+        back(4, late).start()
+        back(1, late).wait_recv()
+        minus_out[low, cols] = (minus_out[low, cols].astype(F32) + far_plus[:, cols].astype(F32)).astype(BF16)
+        back(5, late).start()
+
+    lower_far(0)
+    lower_near(0)
+    for k in range(13, 16):
+        halves.pass_on(k, 1)
+    halves.twin_arrived(3, 0, 16 - EARLY, 1)
+    lower_far(1)
+    add_far(0)
+    lower_near(1)
+    add_far(1)
+    for n, ref in ((4, from_minus), (5, from_plus)):
+        remote(ref, ref, x_send.at[0], x_recv.at[n], plus).wait_recv()
+    lowered = sums[0:own, :] + from_plus[...].astype(F32) + from_minus[...].astype(F32)
+    result = layer_norm(
+        residual_weight * columns(mixed.at[x], chips).astype(F32) + 0.5 * lowered, columns(mlp_gain_ref, chips)
     ).astype(BF16)
+    for n, chip in enumerate(chips):
+        out_ref[:, pl.ds(pl.multiple_of(chip * 2 * depth, 2 * depth), 2 * depth)] = result[:, n * 2 * depth : (n + 1) * 2 * depth]
 
     pieces.sent()
     halves.sent()
@@ -629,8 +671,8 @@
             dma((16, 2)),
             dma((16,)),
             dma((1,)),
-            dma((16, 1)),
-            dma((2,)),
+            dma((16, 2)),
+            dma((4,)),
             dma((1,)),
             dma((7,)),
             dma((2,)),

time: 94.1 us -> 91.3 us (0.970)
  Pallas kernels: 92.1 us -> 89.3 us
    pallas_call x1, Pallas kernels: 92.1 us -> 89.3 us  [per_device(): pl.pallas_call(functools.partial(whole_kernel, rows, const), out_shape=ja...]
where the time goes in v5:
time: 91.3 us; the launch traced here: 91 us
  Pallas kernels  89.3 us (98%)
  local copies, waits for them, and re-layouts  1.77 us (2%)
    pallas_call x1, Pallas kernels, per_device(): pl.pallas_call(functools.partial(whole_kernel, rows, const), out_shape=ja...  89.3 us

profile of v5, /device:TPU:1, one launch (start us, length us, event | category | flops | bytes accessed | tf_op | source)
XLA Modules:
  0.0 91.0 jit_solution(16023835025729369469)
XLA Ops:
  0.0 89.3 %layer.1 = bf16[96,2048]{1,0:T(8,128)(2,1)} custom-call(bf16[384,512]{1,0:T(8,128)(2,1)} %latent_hbm.1, bf16[64,384]{1,0:T(8,128)(2,1)} %bitcast.10, bf16[512,256]{1,0:T(8,128)(2,1)} %key_up_hbm.1, bf16[512,256]{1,0:T(8,128)(2,1)} %value_up_hbm.1, f32[2,32,384]{2,1,0:T(8,128)} %constant.4.clone.inner_hbm, bf16[384,2,128]{2,1,0:T(2,128)(2,1)} %qn_hbm.1, ...), custom_call_target="tpu_custom_call" | custom-call | tf_op jit(solution)/shard_map/layer/pallas_call | solution.py:634
  89.3 1.8 %copy.18 = bf16[96,2048]{1,0:T(8,128)(2,1)} copy(bf16[96,2048]{1,0:T(8,128)(2,1)} %layer.1) | data formatting | bytes 786432

commit v6 on v5

--- a/solution.py
+++ b/solution.py
@@ -264,7 +264,7 @@
             )
         )
     ]
-    for load in loads:
+    for load in loads[:2]:
         load.start()
 
     plus, minus, across = t.along_x(1), t.along_x(-1), t.along_x(2)
@@ -272,10 +272,12 @@
     barrier = pltpu.get_barrier_semaphore()
     for peer in peers:
         pl.semaphore_signal(barrier, inc=1, device_id=peer, device_id_type=MESH)
+    for load in loads[2:]:
+        load.start()
 
     slab_rows = kv.shape[1]
-    pieces = Gather(t, kv, [(0, slab_rows // 2), (slab_rows // 2, slab_rows // 2)], kv_send.at[0], kv_recv, kv_twin, lambda k, part: k)
-    halves = Gather(t, weights, [(0, 2 * depth), (2 * depth, depth)], w_send.at[0], w_recv, w_twin, lambda k, part: 2 * part + k // EARLY)
+    pieces = Gather(t, kv, [(0, 2 * rows), (2 * rows, slab_rows - 2 * rows)], kv_send.at[0], kv_recv, kv_twin, lambda k, part: k)
+    halves = Gather(t, weights, [(0, 2 * depth), (2 * depth, depth)], w_send.at[0], w_recv, w_twin, lambda k, part: k // EARLY if part == 0 else 2 + [first <= k < last for first, last in COLUMN_SETS].index(True))
 
     class Ring:
         def __init__(self, buf, send_sem, first_sem):
@@ -340,16 +342,21 @@
         ref = proj.at[slot, pl.ds(pl.multiple_of(first, share), share)]
         return remote(ref, ref, proj_send.at[0], proj_recv.at[recv], t.twin())
 
-    for load in loads[:6]:
-        load.wait()
+    loads[0].wait()
+    loads[1].wait()
     wide = latent_v[...].astype(F32)
     factor = lax.rsqrt(jnp.mean(wide * wide, axis=-1, keepdims=True) + norm_floor)
     normed = (wide * factor * latent_gain_ref[...]).astype(BF16)
     slab = kv.at[me]
     keys = jnp.dot(normed, key_up_v[...], preferred_element_type=F32).astype(BF16)
+    for h in range(2):
+        slab[h * rows : (h + 1) * rows, :] = keys[:, 128 * h : 128 * (h + 1)]
+    pl.semaphore_wait(barrier, len(peers))
+    pieces.send(0, 0)
+    for load in loads[2:6]:
+        load.wait()
     values = jnp.dot(normed, value_up_v[...], preferred_element_type=F32)
     for h in range(2):
-        slab[h * rows : (h + 1) * rows, :] = keys[:, 128 * h : 128 * (h + 1)]
         turned = values[:, 128 * h : 128 * (h + 1)].T.astype(BF16)
         for i in range(rows // 128):
             at = 2 * rows + h * rows + 128 * i
@@ -362,9 +369,7 @@
     key_turned = turn(rope_key_v[...].astype(F32), cosine, sine).T
     slab[4 * rows : 4 * rows + mid, :] = jnp.concatenate([key_turned[:mid], key_turned[mid:]], axis=1).astype(BF16)
 
-    pl.semaphore_wait(barrier, len(peers))
-    for part in range(2):
-        pieces.send(0, part)
+    pieces.send(0, 1)
     loads[6].wait()
     for copy in proj_first:
         copy.start()
@@ -513,15 +518,12 @@
             u = up_sum[rows_at(d), :] + up[n * own : (n + 1) * own]
             hidden[rows_at(d), :] = (g / (1.0 + jnp.exp(-g)) * u).astype(BF16)
 
-    activate(2, 1)
-    activate(-1, 0)
-    pass_weights(10, 13, 1)
-    halves.twin_arrived(2, 0, EARLY, 1)
-
     half = own // 2
     top, low = pl.ds(0, half), pl.ds(half, half)
-    split = EARLY * 2 * depth
-    column_sets = [(chips[:EARLY], pl.ds(0, split)), (chips[EARLY:], pl.ds(split, sums.shape[1] - split))]
+    column_sets = [
+        (chips[first:last], pl.ds(first * 2 * depth, (last - first) * 2 * depth)) for first, last in COLUMN_SETS
+    ]
+    sets = len(column_sets)
 
     def lower(first, second, late):
         lhs = jnp.concatenate([hidden[rows_at(first), :], hidden[rows_at(second), :]], axis=0)
@@ -534,10 +536,10 @@
         src, src_rows, dst, dst_rows, recv, to = (
             (far_out, top, far_minus, pl.ds(0, half), 2 * late, plus),
             (far_out, low, far_plus, pl.ds(0, half), 2 * late + 1, minus),
-            (plus_out, low, from_minus, low, 4, plus),
-            (minus_out, top, from_plus, top, 5, minus),
-            (plus_out, top, from_minus, top, 4, plus),
-            (minus_out, low, from_plus, low, 5, minus),
+            (plus_out, low, from_minus, low, 2 * sets, plus),
+            (minus_out, top, from_plus, top, 2 * sets + 1, minus),
+            (plus_out, top, from_minus, top, 2 * sets, plus),
+            (minus_out, low, from_plus, low, 2 * sets + 1, minus),
         )[n]
         return remote(src.at[src_rows, cols], dst.at[dst_rows, cols], x_send.at[0], x_recv.at[recv], to)
 
@@ -566,16 +568,27 @@
         minus_out[low, cols] = (minus_out[low, cols].astype(F32) + far_plus[:, cols].astype(F32)).astype(BF16)
         back(5, late).start()
 
+    def down_arrived(n):
+        first, last = COLUMN_SETS[n]
+        halves.twin_arrived(2 + n, 0, last - first, 1)
+
+    activate(2, 1)
+    down_arrived(0)
     lower_far(0)
+    activate(-1, 0)
     lower_near(0)
-    for k in range(13, 16):
-        halves.pass_on(k, 1)
-    halves.twin_arrived(3, 0, 16 - EARLY, 1)
+    pass_weights(10, 13, 1)
+    down_arrived(1)
     lower_far(1)
+    lower_near(1)
     add_far(0)
-    lower_near(1)
+    pass_weights(13, 16, 1)
+    down_arrived(2)
+    lower_far(2)
+    lower_near(2)
     add_far(1)
-    for n, ref in ((4, from_minus), (5, from_plus)):
+    add_far(2)
+    for n, ref in ((2 * sets, from_minus), (2 * sets + 1, from_plus)):
         remote(ref, ref, x_send.at[0], x_recv.at[n], plus).wait_recv()
     lowered = sums[0:own, :] + from_plus[...].astype(F32) + from_minus[...].astype(F32)
     result = layer_norm(
@@ -597,6 +610,7 @@
 
 GROUPS = ((1, 5), (5, 11), (11, 15), (15, 16))
 EARLY = 11
+COLUMN_SETS = ((0, 5), (5, 11), (11, 16))
 PROJ_SECOND = 5
 PROJ_THIRD = 9
 WEIGHTS_FIRST = 12
@@ -672,13 +686,13 @@
             dma((16,)),
             dma((1,)),
             dma((16, 2)),
-            dma((4,)),
+            dma((2 + len(COLUMN_SETS),)),
             dma((1,)),
             dma((7,)),
             dma((2,)),
             dma((12,)),
             dma((1,)),
-            dma((6,)),
+            dma((2 * len(COLUMN_SETS) + 2,)),
         ],
         compiler_params=pltpu.CompilerParams(
             collective_id=0, has_side_effects=True, vmem_limit_bytes=60 * 1024 * 1024

time: 91.3 us -> 89.6 us (0.981)
  Pallas kernels: 89.3 us -> 87.6 us
    pallas_call x1, Pallas kernels: 89.3 us -> 87.6 us  [per_device(): pl.pallas_call(functools.partial(whole_kernel, rows, const), out_shape=ja...]
where the time goes in v6:
time: 89.6 us; the launch traced here: 89.4 us
  Pallas kernels  87.6 us (98%)
  local copies, waits for them, and re-layouts  1.77 us (2%)
    pallas_call x1, Pallas kernels, per_device(): pl.pallas_call(functools.partial(whole_kernel, rows, const), out_shape=ja...  87.6 us

profile of v6, /device:TPU:1, one launch (start us, length us, event | category | flops | bytes accessed | tf_op | source)
XLA Modules:
  0.0 89.4 jit_solution(12216984350034047048)
XLA Ops:
  0.0 87.6 %layer.1 = bf16[96,2048]{1,0:T(8,128)(2,1)} custom-call(bf16[384,512]{1,0:T(8,128)(2,1)} %latent_hbm.1, bf16[64,384]{1,0:T(8,128)(2,1)} %bitcast.10, bf16[512,256]{1,0:T(8,128)(2,1)} %key_up_hbm.1, bf16[512,256]{1,0:T(8,128)(2,1)} %value_up_hbm.1, f32[2,32,384]{2,1,0:T(8,128)} %constant.4.clone.inner_hbm, bf16[384,2,128]{2,1,0:T(2,128)(2,1)} %qn_hbm.1, ...), custom_call_target="tpu_custom_call" | custom-call | tf_op jit(solution)/shard_map/layer/pallas_call | solution.py:648
  87.6 1.8 %copy.18 = bf16[96,2048]{1,0:T(8,128)(2,1)} copy(bf16[96,2048]{1,0:T(8,128)(2,1)} %layer.1) | data formatting | bytes 786432

commit v7 on v6

--- a/solution.py
+++ b/solution.py
@@ -150,7 +150,7 @@
         out = []
         for to, name, which in plan:
             ref = self.ref(slot, part, which)
-            out.append(remote(ref, ref, self.send_sem, self.recv_sems.at[PLACE[name], part], t.at(*to)))
+            out.append(remote(ref, ref, self.send_sem, self.recv_sems.at[PLACE[name] - 1, part], t.at(*to)))
         ref = self.ref(slot, part)
         out.append(remote(ref, ref, self.send_sem, self.twin_sems.at[self.twin_of(k, part)], t.twin()))
         return out
@@ -165,7 +165,7 @@
 
     def arrived(self, k, part):
         ref = self.ref(self.torus.index(*ITEMS[k]), part)
-        remote(ref, ref, self.send_sem, self.recv_sems.at[k, part], self.torus.twin()).wait_recv()
+        remote(ref, ref, self.send_sem, self.recv_sems.at[k - 1, part], self.torus.twin()).wait_recv()
 
     def pass_on(self, k, part):
         self.arrived(k, part)
@@ -245,7 +245,7 @@
     me, x = t.me, t.x
     depth = weights.shape[1] // 3
     loads = [
-        pltpu.make_async_copy(src, dst, load_sems.at[n])
+        pltpu.make_async_copy(src, dst, load_sems.at[min(n, LOADS - 1)])
         for n, (src, dst) in enumerate(
             (
                 (latent_hbm, latent_v),
@@ -257,10 +257,10 @@
                 (proj_hbm, proj.at[x]),
                 (qn_hbm, qn_v),
                 (qr_hbm, qr_v),
-                (down_hbm, weights.at[me, pl.ds(2 * depth, depth)]),
+                (stream_hbm, stream_all.at[x]),
                 (gate_hbm, weights.at[me, pl.ds(0, depth)]),
                 (up_hbm, weights.at[me, pl.ds(depth, depth)]),
-                (stream_hbm, stream_all.at[x]),
+                (down_hbm, weights.at[me, pl.ds(2 * depth, depth)]),
             )
         )
     ]
@@ -293,27 +293,29 @@
                 self.copy(0, 0, 0, plus),
                 self.copy(0, 1, 1, minus),
                 self.copy(0, 1, 2, plus),
-                self.copy(0, 0, 3, minus),
+                self.copy(0, 0, 2, minus),
             ]
 
         def second(self, which):
-            return self.copy(1, 1, 5, minus) if which else self.copy(-1, 0, 4, plus)
+            return self.copy(1, 1, 3, minus) if which else self.copy(-1, 0, 3, plus)
 
         def forward(self):
             for d, which in ((-1, 0), (1, 1)):
                 self.copy(d, which, which, plus).wait_recv()
                 self.second(which).start()
 
+        def both_halves(self, sem):
+            ref = self.buf.at[0]
+            remote(ref, ref, self.send_sem, ring_recv.at[self.first_sem + sem], plus).wait_recv()
+
         def near_arrived(self):
-            self.copy(-1, 1, 2, plus).wait_recv()
-            self.copy(1, 0, 3, plus).wait_recv()
+            self.both_halves(2)
 
         def far_arrived(self):
-            self.copy(2, 0, 4, plus).wait_recv()
-            self.copy(2, 1, 5, plus).wait_recv()
+            self.both_halves(3)
 
     stream_ring = Ring(stream_all, ring_send.at[0], 0)
-    heads_ring = Ring(heads_all, ring_send.at[1], 6)
+    heads_ring = Ring(heads_all, ring_send.at[1], 4)
 
     share = proj.shape[1] // 2
 
@@ -330,17 +332,11 @@
     proj_first = [proj_copy(0, None, 0, 0, plus), proj_copy(0, None, 1, 1, minus)]
     proj_second = [
         proj_copy(-1, 0, 2, 2, plus),
-        proj_copy(1, 1, 3, 3, minus),
-        proj_copy(-1, None, 4, 4, t.twin()),
-        proj_copy(1, None, 5, 5, t.twin()),
+        proj_copy(1, 1, 3, 2, minus),
+        proj_copy(-1, None, 4, 3, t.twin()),
+        proj_copy(1, None, 5, 3, t.twin()),
     ]
-    proj_third = [proj_copy(2, None, 6, 6, t.twin())]
-
-    def twin_proj(d, recv):
-        slot = lax.rem(x + d + 4, 4)
-        first = (1 - t.c) * share
-        ref = proj.at[slot, pl.ds(pl.multiple_of(first, share), share)]
-        return remote(ref, ref, proj_send.at[0], proj_recv.at[recv], t.twin())
+    proj_third = [proj_copy(2, None, 6, 3, t.twin())]
 
     loads[0].wait()
     loads[1].wait()
@@ -374,7 +370,7 @@
     for copy in proj_first:
         copy.start()
 
-    for load in loads[7:]:
+    for load in loads[7 : LOADS - 1]:
         load.wait()
     for copy in stream_ring.first():
         copy.start()
@@ -392,6 +388,7 @@
     acc_ref[...] = jnp.zeros_like(acc_ref)
     attend([kv.at[me]], q_ref, m_ref, l_ref, acc_ref, rows, const, diag=True)
 
+    pltpu.make_async_copy(weights.at[me], weights.at[me], load_sems.at[LOADS - 1]).wait()
     last = len(ITEMS)
 
     def step(i, carry):
@@ -414,8 +411,7 @@
                             for copy in proj_second:
                                 copy.start()
                         if k == PROJ_THIRD:
-                            proj_copy(2, 0, 0, 2, minus).wait_recv()
-                            proj_copy(2, 1, 0, 3, minus).wait_recv()
+                            proj_copy(2, None, 0, 2, minus).wait_recv()
                             for copy in proj_third:
                                 copy.start()
                             stream_ring.forward()
@@ -461,8 +457,8 @@
     pass_weights(1, 5, 0)
     stream_ring.near_arrived()
     stream_ring.far_arrived()
-    for d, sem in ((1, 4), (-1, 5), (2, 6)):
-        twin_proj(d, sem).wait_recv()
+    twin_proj = proj.at[pl.ds(0, 3), pl.ds(0, share)]
+    remote(twin_proj, twin_proj, proj_send.at[0], proj_recv.at[3], t.twin()).wait_recv()
     heads_ring.forward()
     pass_weights(5, 8, 0)
     heads_ring.near_arrived()
@@ -609,11 +605,12 @@
 
 
 GROUPS = ((1, 5), (5, 11), (11, 15), (15, 16))
+LOADS = 11
 EARLY = 11
 COLUMN_SETS = ((0, 5), (5, 11), (11, 16))
 PROJ_SECOND = 5
 PROJ_THIRD = 9
-WEIGHTS_FIRST = 12
+WEIGHTS_FIRST = 13
 
 
 def per_device(
@@ -680,17 +677,17 @@
             pltpu.VMEM((own // 2, width), BF16),
             pltpu.VMEM((own, width), BF16),
             pltpu.VMEM((own, width), BF16),
-            dma((13,)),
+            dma((LOADS,)),
             dma((1,)),
-            dma((16, 2)),
+            dma((15, 2)),
             dma((16,)),
             dma((1,)),
-            dma((16, 2)),
+            dma((15, 2)),
             dma((2 + len(COLUMN_SETS),)),
             dma((1,)),
-            dma((7,)),
+            dma((4,)),
             dma((2,)),
-            dma((12,)),
+            dma((8,)),
             dma((1,)),
             dma((2 * len(COLUMN_SETS) + 2,)),
         ],

time: 89.6 us -> 89 us (level)
  no operation moved by 1% of the time
where the time goes in v7:
time: 89 us; the launch traced here: 88.8 us
  Pallas kernels  87 us (98%)
  local copies, waits for them, and re-layouts  1.77 us (2%)
    pallas_call x1, Pallas kernels, per_device(): pl.pallas_call(functools.partial(whole_kernel, rows, const), out_shape=ja...  87 us

profile of v7, /device:TPU:1, one launch (start us, length us, event | category | flops | bytes accessed | tf_op | source)
XLA Modules:
  0.0 88.8 jit_solution(2781797750042681424)
XLA Ops:
  0.0 87.0 %layer.1 = bf16[96,2048]{1,0:T(8,128)(2,1)} custom-call(bf16[384,512]{1,0:T(8,128)(2,1)} %latent_hbm.1, bf16[64,384]{1,0:T(8,128)(2,1)} %bitcast.10, bf16[512,256]{1,0:T(8,128)(2,1)} %key_up_hbm.1, bf16[512,256]{1,0:T(8,128)(2,1)} %value_up_hbm.1, f32[2,32,384]{2,1,0:T(8,128)} %constant.4.clone.inner_hbm, bf16[384,2,128]{2,1,0:T(2,128)(2,1)} %qn_hbm.1, ...), custom_call_target="tpu_custom_call" | custom-call | tf_op jit(solution)/shard_map/layer/pallas_call | solution.py:645
  87.0 1.8 %copy.18 = bf16[96,2048]{1,0:T(8,128)(2,1)} copy(bf16[96,2048]{1,0:T(8,128)(2,1)} %layer.1) | data formatting | bytes 786432

commit v8 on v7

--- a/solution.py
+++ b/solution.py
@@ -288,13 +288,9 @@
             n = self.first_sem + sem
             return remote(ref, ref, self.send_sem, ring_recv.at[n], to)
 
-        def first(self):
-            return [
-                self.copy(0, 0, 0, plus),
-                self.copy(0, 1, 1, minus),
-                self.copy(0, 1, 2, plus),
-                self.copy(0, 0, 2, minus),
-            ]
+        def first(self, begin=0, end=4):
+            plan = ((0, 0, plus), (1, 1, minus), (1, 2, plus), (0, 2, minus))
+            return [self.copy(0, *one) for one in plan[begin:end]]
 
         def second(self, which):
             return self.copy(1, 1, 3, minus) if which else self.copy(-1, 0, 3, plus)
@@ -447,7 +443,7 @@
     own = rows // 4
     for h in range(2):
         heads_all[x, :, 128 * h : 128 * (h + 1)] = (acc_ref[h] / l_ref[h]).T.astype(BF16)
-    for copy in heads_ring.first():
+    for copy in heads_ring.first(0, 2):
         copy.start()
 
     def pass_weights(first, last, part):
@@ -459,6 +455,8 @@
     stream_ring.far_arrived()
     twin_proj = proj.at[pl.ds(0, 3), pl.ds(0, share)]
     remote(twin_proj, twin_proj, proj_send.at[0], proj_recv.at[3], t.twin()).wait_recv()
+    for copy in heads_ring.first(2, 4):
+        copy.start()
     heads_ring.forward()
     pass_weights(5, 8, 0)
     heads_ring.near_arrived()

time: 89 us -> 89 us (level)
  no operation moved by 1% of the time
where the time goes in v8:
time: 89 us; the launch traced here: 88.8 us
  Pallas kernels  87 us (98%)
  local copies, waits for them, and re-layouts  1.77 us (2%)
    pallas_call x1, Pallas kernels, per_device(): pl.pallas_call(functools.partial(whole_kernel, rows, const), out_shape=ja...  87 us

profile of v8, /device:TPU:1, one launch (start us, length us, event | category | flops | bytes accessed | tf_op | source)
XLA Modules:
  0.0 88.8 jit_solution(13876702824500166947)
XLA Ops:
  0.0 87.0 %layer.1 = bf16[96,2048]{1,0:T(8,128)(2,1)} custom-call(bf16[384,512]{1,0:T(8,128)(2,1)} %latent_hbm.1, bf16[64,384]{1,0:T(8,128)(2,1)} %bitcast.10, bf16[512,256]{1,0:T(8,128)(2,1)} %key_up_hbm.1, bf16[512,256]{1,0:T(8,128)(2,1)} %value_up_hbm.1, f32[2,32,384]{2,1,0:T(8,128)} %constant.4.clone.inner_hbm, bf16[384,2,128]{2,1,0:T(2,128)(2,1)} %qn_hbm.1, ...), custom_call_target="tpu_custom_call" | custom-call | tf_op jit(solution)/shard_map/layer/pallas_call | solution.py:643
  87.0 1.8 %copy.18 = bf16[96,2048]{1,0:T(8,128)(2,1)} copy(bf16[96,2048]{1,0:T(8,128)(2,1)} %layer.1) | data formatting | bytes 786432
